TPU v7x, 32 devices: a whole 2x2x4 slice. The times are simulated.
32 devices in a mesh: sp: 8 (over z, x), tp: 4 (over y, core).
Axes of the slice: x: 2, y: 2, z: 4, core: 2. Of those that a mesh axis runs over, the one named last changes fastest.
Arguments:
- features: bfloat16 [3072, 2048], P('sp', 'tp'), may hold values from -6 to 6
- norm_gain: float32 [2048], replicated, may hold values from 0.28 to 10
- w_query: bfloat16 [2048, 1024], P(None, 'tp'), may hold values from -0.125 to 0.125
- w_key: bfloat16 [2048, 512], P(None, 'tp'), may hold values from -0.125 to 0.125
- w_value: bfloat16 [2048, 512], P(None, 'tp'), may hold values from -0.125 to 0.125
- head_sinks: float32 [16], P('tp'), may hold values from 1 to 5
- w_query_latent: bfloat16 [2048, 512], replicated, may hold values from -0.125 to 0.125
- w_kv_latent: bfloat16 [2048, 512], replicated, may hold values from -0.125 to 0.125
- w_rope_key: bfloat16 [2048, 64], replicated, may hold values from -0.125 to 0.125
- query_latent_gain: float32 [512], replicated, may hold values from 0.28 to 10
- kv_latent_gain: float32 [512], replicated, may hold values from 0.28 to 10
- w_query_content: bfloat16 [512, 1024], P(None, 'tp'), may hold values from -0.25 to 0.25
- w_query_rotary: bfloat16 [512, 512], P(None, 'tp'), may hold values from -0.25 to 0.25
- w_key_up: bfloat16 [512, 1024], P(None, 'tp'), may hold values from -0.25 to 0.25
- w_value_up: bfloat16 [512, 1024], P(None, 'tp'), may hold values from -0.25 to 0.25
- w_branch_window: bfloat16 [1024, 2048], P('tp'), may hold values from -0.1875 to 0.1875
- w_branch_latent: bfloat16 [1024, 2048], P('tp'), may hold values from -0.1875 to 0.1875
- w_gate_window: bfloat16 [2048, 2048], P(None, 'tp'), may hold values from -0.125 to 0.125
- w_gate_latent: bfloat16 [2048, 2048], P(None, 'tp'), may hold values from -0.125 to 0.125
Outputs:
- mixed: bfloat16 [3072, 2048], P('sp', 'tp')
All inputs are finite; a program needn't handle non-finite values.
Results may differ from a plain program's by a relative error of at most 0.018.
The roundings to bfloat16 on the way count: a program that leaves them out, or rounds other values in their place, can miss the bound.
Values may be sent and summed in bfloat16 or wider, within the bound.
A program may use at most 128 MiB of HBM per device.

v0:
```python
import functools

import jax
import jax.numpy as jnp
from jax import lax
from jax.experimental import pallas as pl
from jax.experimental.pallas import tpu as pltpu
from jax.sharding import PartitionSpec as P

HEAD = 64
WINDOW = 128
NOPE = 128
ROPE = 64
VDIM = 128


EPS = 1e-06
THETA = 10000.0
NEGATIVE = -1e30
LANES = 128
LOG2_E = 1.4426950408889634
MESH = pl.DeviceIdType.MESH
BF16 = jnp.bfloat16
F32 = jnp.float32


def dot(left, right):
    return jnp.dot(left, right, preferred_element_type=F32)


def dot_t(left, right):
    return lax.dot_general(left, right, (((1,), (1,)), ((), ())), preferred_element_type=F32)


def rms_rows(rows, gain):
    return rows * lax.rsqrt(jnp.mean(rows * rows, axis=-1, keepdims=True) + EPS) * gain


def swap_halves(rows):
    half = rows.shape[1] // 2
    return jnp.concatenate([rows[:, half:], rows[:, :half]], axis=1)


WEIGHTS = (
    "kv_latent", "rope", "key", "value", "query", "query_latent", "content", "rotary",
    "key_up", "value_up", "gate_window", "gate_latent",
)


def kernel(dims, *refs):
    n_sp, n_tp, n_x = dims
    n_z, n_y = n_sp // n_x, n_tp // 2
    features, norm_gain, sinks, q_gain, kv_gain, frequency = refs[:6]
    refs = (None,) + refs
    w_hbm = dict(zip(WEIGHTS, refs[7:19]))
    branch_hbm = refs[19:21]
    out = refs[21]
    feat, normed, wide = refs[22:25]
    w = dict(zip(WEIGHTS, refs[25:37]))
    columns = refs[37:39]
    kvb, local_kv, halo, queries, q_full, gates, win, lat, top, total, acc = refs[39:50]
    w_sem, own_sem, col_own, col_send, col_recv, halo_sem, y_send, y_recv, s_send, s_recv = refs[50:60]
    z_send, z_recv, x_send, x_recv, c_send, c_recv, d_send, d_recv = refs[60:68]
    cosine, sine = refs[68:70]

    sp, tp = lax.axis_index("sp"), lax.axis_index("tp")
    z, x = sp // n_x, lax.rem(sp, n_x)
    y, core = tp // 2, lax.rem(tp, 2)
    sibling = y * 2 + (1 - core)
    rows, block = features.shape
    half = rows // 2
    lat_heads = w_hbm["key_up"].shape[1] // NOPE
    kv_width = w_hbm["key"].shape[1]
    kv_heads = kv_width // HEAD
    group = w_hbm["query"].shape[1] // kv_width
    latent = w_hbm["kv_latent"].shape[1]

    loads = {}
    own_feat = [
        pltpu.make_async_copy(features.at[pl.ds(h * half, half)], feat.at[tp, h], own_sem.at[h])
        for h in range(2)
    ]
    for copy in own_feat:
        copy.start()
    for i, name in enumerate(WEIGHTS):
        loads[name] = pltpu.make_async_copy(w_hbm[name], w[name], w_sem.at[i])
        loads[name].start()

    def remote(src, dst, send, recv, where):
        return pltpu.make_async_remote_copy(
            src_ref=src, dst_ref=dst, send_sem=send, recv_sem=recv,
            device_id=where, device_id_type=MESH,
        )

    barrier = pltpu.get_barrier_semaphore()

    def greet(where):
        pl.semaphore_signal(barrier, inc=1, device_id=where, device_id_type=MESH)

    for d in range(1, n_tp):
        greet({"sp": sp, "tp": lax.rem(tp + d, n_tp)})
    for d in range(1, n_x):
        greet({"sp": z * n_x + lax.rem(x + d, n_x), "tp": tp})

    @pl.when(z + 1 < n_z)
    def _():
        greet({"sp": sp + n_x, "tp": tp})

    @pl.when(z > 0)
    def _():
        greet({"sp": sp - n_x, "tp": tp})

    @pl.when(sp + 1 < n_sp)
    def _():
        greet({"sp": sp + 1, "tp": tp})

    @pl.when(sp > 0)
    def _():
        greet({"sp": sp - 1, "tp": tp})

    one, none = jnp.int32(1), jnp.int32(0)
    pl.semaphore_wait(
        barrier,
        n_tp - 1 + n_x - 1
        + jnp.where(z + 1 < n_z, one, none) + jnp.where(z > 0, one, none)
        + jnp.where(sp + 1 < n_sp, one, none) + jnp.where(sp > 0, one, none),
    )

    def gather(view, which):
        own = view(tp)
        sends = [
            remote(own, own, y_send.at[which, d], y_recv.at[which, d],
                   {"sp": sp, "tp": lax.rem(y + d, n_y) * 2 + core})
            for d in range(1, n_y)
        ]
        sends.append(remote(own, own, s_send.at[which, 0], s_recv.at[which, 0],
                            {"sp": sp, "tp": sibling}))
        return sends

    def start(copies):
        for copy in copies:
            copy.start()

    def forward(view, which):
        for d in range(1, n_y):
            ref = view(lax.rem(y + n_y - d, n_y) * 2 + core)
            remote(ref, ref, y_send.at[which, d], y_recv.at[which, d],
                   {"sp": sp, "tp": sibling}).wait_recv()
            remote(ref, ref, s_send.at[which, d], s_recv.at[which, d],
                   {"sp": sp, "tp": sibling}).start()

    def arrived(view, which):
        for d in range(n_y):
            ref = view(lax.rem(y + n_y - d, n_y) * 2 + (1 - core))
            remote(ref, ref, s_send.at[which, d], s_recv.at[which, d],
                   {"sp": sp, "tp": sibling}).wait_recv()

    def sent(view, which):
        own = view(tp)
        for d in range(1, n_y):
            remote(own, own, y_send.at[which, d], y_recv.at[which, d],
                   {"sp": sp, "tp": sibling}).wait_send()
        for d in range(n_y):
            remote(own, own, s_send.at[which, d], s_recv.at[which, d],
                   {"sp": sp, "tp": sibling}).wait_send()

    feat_half = [lambda slot, h=h: feat.at[slot, h] for h in range(2)]
    lat_half = [lambda slot, h=h: lat.at[slot, h] for h in range(2)]
    win_all = lambda slot: win.at[slot]

    for h in range(2):
        own_feat[h].wait()
        start(gather(feat_half[h], h))

    positions = (sp * rows + lax.broadcasted_iota(jnp.int32, (rows, ROPE), 0)).astype(F32)
    angles = positions * frequency[...]
    lane = lax.broadcasted_iota(jnp.int32, (rows, ROPE), 1)
    cosine[...] = jnp.cos(angles)
    turned = jnp.sin(angles)
    sine[...] = jnp.where(lane < ROPE // 2, -turned, turned)

    def column_copies():
        local, sends = [], []
        for b in range(2):
            span = branch_hbm[b]
            local.append(pltpu.make_async_copy(
                span.at[:, pl.ds(pl.multiple_of(tp * block, LANES), block)],
                columns[b].at[tp], col_own.at[b]))
            for d in range(1, n_tp):
                to = lax.rem(tp + d, n_tp)
                sends.append(remote(
                    span.at[:, pl.ds(pl.multiple_of(to * block, LANES), block)],
                    columns[b].at[tp], col_send.at[b, d], col_recv.at[b, d],
                    {"sp": sp, "tp": to}))
        return local, sends

    column_local, column_sends = column_copies()

    def normalize(h):
        squares = jnp.zeros((half, 1), F32)
        for j in range(n_tp):
            piece = feat[j, h].astype(F32)
            squares = squares + jnp.sum(piece * piece, axis=-1, keepdims=True)
        scale = lax.rsqrt(squares / (n_tp * block) + EPS)
        for j in range(n_tp):
            span = slice(j * block, (j + 1) * block)
            piece = feat[j, h].astype(F32) * scale * norm_gain[:, span]
            normed[h * half : (h + 1) * half, span] = piece.astype(BF16)

    def wide_dot(name, at):
        tile = min(256, latent)

        def step(i, _):
            to = pl.ds(pl.multiple_of(i * tile, LANES), tile)
            wide[at, to] = dot(normed[at, :], w[name][:, to])
            return 0

        lax.fori_loop(0, w[name].shape[1] // tile, step, 0)

    padding = jnp.zeros((rows, LANES - ROPE), F32)

    def latents(h):
        at = slice(h * half, (h + 1) * half)
        wide_dot("kv_latent", at)
        rope = dot_t(normed[at, :], w["rope"][...])
        rope = rope * cosine[at, :] + swap_halves(rope) * sine[at, :]
        rope = jnp.concatenate([rope, padding[at]], axis=1).astype(BF16)
        kvb[sp, h, :, :, :latent] = (
            rms_rows(wide[at, :], kv_gain[...]).astype(BF16).reshape(2, half // 2, latent))
        kvb[sp, h, :, :, latent:] = rope.reshape(2, half // 2, LANES)

    def column_slot(k):
        return (z - k) * n_x + x

    def row_slot(k, d):
        return (z - k) * n_x + lax.rem(x + n_x - d, n_x)

    def z_copy(k, h):
        ref = kvb.at[column_slot(k), h, core]
        return remote(ref, ref, z_send.at[h, k], z_recv.at[h, k + 1], {"sp": sp + n_x, "tp": tp})

    def x_copy(k, d, h):
        ref = kvb.at[column_slot(k), h, core]
        return remote(ref, ref, x_send.at[h, k, d], x_recv.at[h, k, d],
                      {"sp": z * n_x + lax.rem(x + d, n_x), "tp": tp})

    def c_copy(k, h, which):
        ref = kvb.at[column_slot(k), h, which]
        return remote(ref, ref, c_send.at[h, k], c_recv.at[h, k], {"sp": sp, "tp": sibling})

    def d_copy(k, d, h, which):
        ref = kvb.at[row_slot(k, d), h, which]
        return remote(ref, ref, d_send.at[h, k, d], d_recv.at[h, k, d],
                      {"sp": sp, "tp": sibling})

    def pass_on(k, h):
        @pl.when(z + 1 < n_z)
        def _():
            z_copy(k, h).start()

        for d in range(1, n_x):
            x_copy(k, d, h).start()

    def take_column(k):
        for h in range(2):
            ref = kvb.at[column_slot(k), h, core]
            remote(ref, ref, z_send.at[h, k], z_recv.at[h, k],
                   {"sp": sp, "tp": sibling}).wait_recv()
            pass_on(k, h)
            c_copy(k, h, core).start()

    def take_rows(k):
        for h in range(2):
            for d in range(1, n_x):
                ref = kvb.at[row_slot(k, d), h, core]
                remote(ref, ref, x_send.at[h, k, d], x_recv.at[h, k, d],
                       {"sp": sp, "tp": sibling}).wait_recv()
                d_copy(k, d, h, core).start()

    loads["kv_latent"].wait()
    loads["rope"].wait()
    for h in range(2):
        forward(feat_half[h], h)
        arrived(feat_half[h], h)
        if h == 1:
            start(column_local)
            start(column_sends)
        normalize(h)
        latents(h)
        pass_on(0, h)

    loads["key"].wait()
    loads["value"].wait()
    local_kv[:, :kv_width] = dot(normed[...], w["key"][...]).astype(BF16)
    local_kv[:, kv_width:] = dot(normed[...], w["value"][...]).astype(BF16)
    tail = local_kv.at[pl.ds(rows - WINDOW, WINDOW)]
    halo_copy = remote(tail, halo, halo_sem.at[0], halo_sem.at[1], {"sp": sp + 1, "tp": tp})

    @pl.when(sp + 1 < n_sp)
    def _():
        halo_copy.start()

    loads["query"].wait()
    queries[...] = dot(normed[...], w["query"][...]).astype(BF16)

    loads["query_latent"].wait()
    wide_dot("query_latent", slice(0, rows))
    latent_query = rms_rows(wide[...], q_gain[...]).astype(BF16)
    loads["content"].wait()
    loads["rotary"].wait()
    content = dot(latent_query, w["content"][...]).astype(BF16)
    rotary = dot(latent_query, w["rotary"][...])
    for h in range(lat_heads):
        turned = rotary[:, h * ROPE : (h + 1) * ROPE]
        turned = turned * cosine[...] + swap_halves(turned) * sine[...]
        q_full[h, :, :NOPE] = content[:, h * NOPE : (h + 1) * NOPE]
        q_full[h, :, NOPE:] = jnp.concatenate([turned, padding], axis=1).astype(BF16)
    loads["key_up"].wait()
    loads["value_up"].wait()

    def attend(slot, diagonal):
        both = kvb[slot].reshape(rows, latent + LANES)
        source, rope_part = both[:, :latent], both[:, latent:]
        keys = dot(source, w["key_up"][...]).astype(BF16)
        values = dot(source, w["value_up"][...]).astype(BF16)
        for h in range(lat_heads):
            key = jnp.concatenate([keys[:, h * NOPE : (h + 1) * NOPE], rope_part], axis=1)
            scores = dot_t(q_full[h], key) * ((NOPE + ROPE) ** (-0.5) * LOG2_E)
            if diagonal:
                live = (lax.broadcasted_iota(jnp.int32, scores.shape, 1)
                        <= lax.broadcasted_iota(jnp.int32, scores.shape, 0))
                scores = jnp.where(live, scores, NEGATIVE)
            peak = jnp.max(scores, axis=-1, keepdims=True)
            if not diagonal:
                before = top[h][:, :1]
                peak = jnp.maximum(peak, before)
                fade = jnp.exp2(before - peak)
            weights = jnp.exp2(scores - peak)
            weight_sum = jnp.sum(weights, axis=-1, keepdims=True)
            part = dot(weights.astype(BF16), values[:, h * VDIM : (h + 1) * VDIM])
            if not diagonal:
                weight_sum = total[h][:, :1] * fade + weight_sum
                part = acc[h] * fade + part
            top[h] = jnp.broadcast_to(peak, (rows, LANES))
            total[h] = jnp.broadcast_to(weight_sum, (rows, LANES))
            acc[h] = part

    def window():
        @pl.when(sp > 0)
        def _():
            remote(tail, halo, halo_sem.at[0], halo_sem.at[1],
                   {"sp": sp, "tp": sibling}).wait_recv()

        @pl.when(sp == 0)
        def _():
            halo[...] = jnp.zeros(halo.shape, BF16)

        row = lax.broadcasted_iota(jnp.int32, (WINDOW, 2 * WINDOW), 0)
        column = lax.broadcasted_iota(jnp.int32, (WINDOW, 2 * WINDOW), 1)
        offset = row + WINDOW - column
        in_band = (offset >= 0) & (offset < WINDOW)
        for n in range(rows // WINDOW):
            at = slice(n * WINDOW, (n + 1) * WINDOW)
            earlier = halo[...] if n == 0 else local_kv[(n - 1) * WINDOW : n * WINDOW]
            band = jnp.concatenate([earlier, local_kv[at]], axis=0)
            valid = in_band & (sp * rows + n * WINDOW + column - WINDOW >= 0)
            heads = []
            for g in range(kv_heads):
                key = band[:, g * HEAD : (g + 1) * HEAD]
                value = band[:, kv_width + g * HEAD : kv_width + (g + 1) * HEAD]
                for i in range(group):
                    q = g * group + i
                    scores = dot_t(queries[at, q * HEAD : (q + 1) * HEAD], key) * HEAD ** (-0.5)
                    scores = jnp.where(valid, scores, NEGATIVE)
                    sink = sinks[0, q]
                    peak = jnp.maximum(jnp.max(scores, axis=-1, keepdims=True), sink)
                    weights = jnp.exp(scores - peak)
                    bottom = jnp.sum(weights, axis=-1, keepdims=True) + jnp.exp(sink - peak)
                    heads.append(dot((weights / bottom).astype(BF16), value))
            win[tp, at, :] = jnp.concatenate(heads, axis=1).astype(BF16)

    def gate(b):
        name = WEIGHTS[10 + b]
        loads[name].wait()

        def step(i, _):
            at = pl.ds(pl.multiple_of(i * 256, LANES), 256)
            gates[b, :, at] = jax.nn.sigmoid(dot(normed[...], w[name][:, at]))
            return 0

        lax.fori_loop(0, block // 256, step, 0)

    def step(k, _):
        @pl.when((z >= k) & (k < n_z))
        def _():
            take_column(k)

        @pl.when(k == 1)
        def _():
            attend(sp, True)

        @pl.when(k == 2)
        def _():
            window()
            start(gather(win_all, 2))

        @pl.when((k > 1) & (z >= k - 1))
        def _():
            for h in range(2):
                c_copy(k - 1, h, 1 - core).wait_recv()
            attend(column_slot(k - 1), False)

        @pl.when(z >= k - 1)
        def _():
            take_rows(k - 1)

        for d in range(1, n_x):
            @pl.when(z >= k - 1)
            def _():
                for h in range(2):
                    d_copy(k - 1, d, h, 1 - core).wait_recv()

            @pl.when((z >= k - 1) & ((k > 1) | (lax.rem(x + n_x - d, n_x) < x)))
            def _():
                attend(row_slot(k - 1, d), False)

        return 0

    lax.fori_loop(1, max(n_z, 2) + 1, step, 0)

    for part in range(2):
        at = slice(part * half, (part + 1) * half)
        for h in range(lat_heads):
            lat[tp, part, :, h * VDIM : (h + 1) * VDIM] = (
                acc[h, at] / total[h, at][:, :1]).astype(BF16)
        start(gather(lat_half[part], 3 + part))
    gate(0)
    forward(win_all, 2)
    gate(1)
    arrived(win_all, 2)
    for copy in column_local:
        copy.wait()
    for b in range(2):
        for d in range(1, n_tp):
            source = lax.rem(tp + n_tp - d, n_tp)
            ref = columns[b].at[source]
            remote(ref, ref, col_send.at[b, d], col_recv.at[b, d],
                   {"sp": sp, "tp": sibling}).wait_recv()
    window_branch = jnp.zeros((rows, block), F32)
    for j in range(n_tp):
        window_branch = window_branch + dot(win[j], columns[0][j])
    gates[0] = gates[0] * window_branch
    for part in range(2):
        at = slice(part * half, (part + 1) * half)
        forward(lat_half[part], 3 + part)
        arrived(lat_half[part], 3 + part)
        latent_branch = jnp.zeros((half, block), F32)
        for j in range(n_tp):
            latent_branch = latent_branch + dot(lat[j, part], columns[1][j])
        out[at, :] = (gates[0, at] + gates[1, at] * latent_branch).astype(BF16)

    for which, view in enumerate((*feat_half, win_all, *lat_half)):
        sent(view, which)
    for copy in column_sends:
        copy.wait_send()

    @pl.when(sp + 1 < n_sp)
    def _():
        halo_copy.wait_send()

    def drain(k, _):
        @pl.when(z >= k)
        def _():
            for h in range(2):
                @pl.when(z + 1 < n_z)
                def _():
                    z_copy(k, h).wait_send()

                for d in range(1, n_x):
                    x_copy(k, d, h).wait_send()
                    d_copy(k, d, h, core).wait_send()

                @pl.when(k > 0)
                def _():
                    c_copy(k, h, core).wait_send()

        return 0

    lax.fori_loop(0, n_z, drain, 0)


def on_device(dims, features, norm_gain, w_query, w_key, w_value, head_sinks, w_query_latent,
              w_kv_latent, w_rope_key, query_latent_gain, kv_latent_gain, w_query_content,
              w_query_rotary, w_key_up, w_value_up, w_branch_window, w_branch_latent,
              w_gate_window, w_gate_latent):
    n_sp, n_tp, n_x = dims
    n_z, n_y = n_sp // n_x, n_tp // 2
    rows, block = features.shape
    width = norm_gain.shape[0]
    latent = w_kv_latent.shape[1]
    lat_heads = w_key_up.shape[1] // NOPE
    half_width = ROPE // 2
    entry = lax.rem(jnp.arange(ROPE, dtype=jnp.int32), half_width).astype(F32)
    frequency = (THETA ** (-entry / half_width))[None, :]
    weights = (w_kv_latent, w_rope_key.T, w_key, w_value, w_query, w_query_latent, w_query_content,
               w_query_rotary, w_key_up, w_value_up, w_gate_window, w_gate_latent)
    branches = (w_branch_window, w_branch_latent)
    vmem = pl.BlockSpec(memory_space=pltpu.VMEM)
    hbm = pl.BlockSpec(memory_space=pl.ANY)
    dma = pltpu.SemaphoreType.DMA
    return pl.pallas_call(
        functools.partial(kernel, dims),
        out_shape=jax.ShapeDtypeStruct((rows, block), BF16),
        in_specs=[hbm, vmem, pl.BlockSpec(memory_space=pltpu.SMEM), vmem, vmem, vmem]
        + [hbm] * (len(weights) + 2),
        out_specs=vmem,
        scratch_shapes=[
            pltpu.VMEM((n_tp, 2, rows // 2, block), BF16),
            pltpu.VMEM((rows, width), BF16),
            pltpu.VMEM((rows, latent), F32),
            *[pltpu.VMEM(weight.shape, BF16) for weight in weights],
            *[pltpu.VMEM((n_tp, branch.shape[0], block), BF16) for branch in branches],
            pltpu.VMEM((n_sp, 2, 2, rows // 4, latent + LANES), BF16),
            pltpu.VMEM((rows, 2 * w_key.shape[1]), BF16),
            pltpu.VMEM((WINDOW, 2 * w_key.shape[1]), BF16),
            pltpu.VMEM((rows, w_query.shape[1]), BF16),
            pltpu.VMEM((lat_heads, rows, NOPE + LANES), BF16),
            pltpu.VMEM((2, rows, block), F32),
            pltpu.VMEM((n_tp, rows, w_query.shape[1]), BF16),
            pltpu.VMEM((n_tp, 2, rows // 2, lat_heads * VDIM), BF16),
            *[pltpu.VMEM((lat_heads, rows, LANES), F32)] * 3,
            dma((len(weights),)),
            dma((2,)),
            dma((2,)),
            dma((2, n_tp)),
            dma((2, n_tp)),
            dma((2,)),
            *[dma((5, n_y))] * 4,
            dma((2, n_z + 1)),
            dma((2, n_z + 1)),
            dma((2, n_z, n_x)),
            dma((2, n_z, n_x)),
            dma((2, n_z)),
            dma((2, n_z)),
            dma((2, n_z, n_x)),
            dma((2, n_z, n_x)),
            *[pltpu.VMEM((rows, ROPE), F32)] * 2,
        ],
        compiler_params=pltpu.CompilerParams(
            collective_id=0, has_side_effects=True, vmem_limit_bytes=60 * 1024 * 1024
        ),
    )(features, norm_gain[None, :], head_sinks[None, :], query_latent_gain[None, :],
      kv_latent_gain[None, :], frequency, *weights, *branches)


def solution(mesh):
    n_sp, n_tp = mesh.shape["sp"], mesh.shape["tp"]
    n_x = 1
    while n_sp % (2 * n_x) == 0 and 8 * n_x * n_x <= n_sp:
        n_x *= 2
    return jax.shard_map(
        functools.partial(on_device, (n_sp, n_tp, n_x)),
        mesh=mesh,
        in_specs=(
            P("sp", "tp"),
            P(),
            P(None, "tp"),
            P(None, "tp"),
            P(None, "tp"),
            P("tp"),
            P(),
            P(),
            P(),
            P(),
            P(),
            P(None, "tp"),
            P(None, "tp"),
            P(None, "tp"),
            P(None, "tp"),
            P("tp", None),
            P("tp", None),
            P(None, "tp"),
            P(None, "tp"),
        ),
        out_specs=P("sp", "tp"),
        check_vma=False,
    )
```

profile of v0, /device:TPU:25, one launch (start us, length us, event | category | flops | bytes accessed | tf_op | source)
XLA Modules:
  0.0 60.0 jit_solution(4052148196184801607)
XLA Ops:
  0.0 0.5 multiply_power_fusion.refs_5_
  0.5 57.7 %shard_map.181 = bf16[384,512]{1,0:T(8,128)(2,1)} custom-call(bf16[384,512]{1,0:T(8,128)(2,1)} %refs_0_.1, f32[1,2048]{1,0:T(1,128)} %bitcast.6, f32[1,4]{1,0:T(1,128)} %bitcast.9, f32[1,512]{1,0:T(1,128)} %bitcast.7, f32[1,512]{1,0:T(1,128)} %bitcast.8, f32[1,64]{1,0:T(1,128)} %multiply_power_fusion.refs_5_, bf16[2048,512]{1,0:T(8,128)(2,1)} %refs_6_.1, ...), custom_call_target="tpu_custom_call" | custom-call | tf_op jit(solution)/shard_map/pallas_call | solution.py:511
  58.2 1.8 %copy.21 = bf16[384,512]{1,0:T(8,128)(2,1)} copy(bf16[384,512]{1,0:T(8,128)(2,1)} %shard_map.181) | data formatting | bytes 786432
where the time goes:
time: 60.3 us; the launch traced here: 60 us
  Pallas kernels  57.7 us (96%)
  local copies, waits for them, and re-layouts  1.77 us (3%)
    pallas_call x1, Pallas kernels, on_device(): pl.pallas_call(functools.partial(kernel, dims), out_shape=jax.ShapeDtypeS...  57.7 us
    unnamed x1, local copies, waits for them, and re-layouts  1.77 us

commit v1 on v0

v1 whole, which is shorter than its diff:
```python
import functools
import types

import jax
import jax.numpy as jnp
import numpy as np
from jax import lax
from jax.experimental import pallas as pl
from jax.experimental.pallas import tpu as pltpu
from jax.sharding import PartitionSpec as P

HEAD = 64
WINDOW = 128
NOPE = 128
ROPE = 64
VDIM = 128


EPS = 1e-06
THETA = 10000.0
NEGATIVE = -1e30
LANES = 128
LOG2_E = 1.4426950408889634
MESH = pl.DeviceIdType.MESH
BF16 = jnp.bfloat16
F32 = jnp.float32
PIECES = 4


def dot(left, right):
    return jnp.dot(left, right, preferred_element_type=F32)


def dot_t(left, right):
    return lax.dot_general(left, right, (((1,), (1,)), ((), ())), preferred_element_type=F32)


def dot_tl(left, right):
    return lax.dot_general(left, right, (((0,), (0,)), ((), ())), preferred_element_type=F32)


def rms_rows(rows, gain):
    return rows * lax.rsqrt(jnp.mean(rows * rows, axis=-1, keepdims=True) + EPS) * gain


def swap_halves(rows):
    half = rows.shape[1] // 2
    return jnp.concatenate([rows[:, half:], rows[:, :half]], axis=1)


SMALL = ("norm_gain", "sinks", "q_gain", "kv_gain", "frequency")
WEIGHTS = (
    "kv_latent", "rope", "key", "value", "query", "query_latent", "content", "rotary",
    "key_up", "value_up", "gate_window", "gate_latent",
)
def bundle(names, values):
    return types.SimpleNamespace(**dict(zip(names, values)))


MERGED = ("key", "value", "query")


def kernel(dims, names, *refs):
    n_sp, n_tp, n_x = dims
    n_z, n_y = n_sp // n_x, n_tp // 2
    features = refs[0]
    small_hbm = bundle(SMALL, refs[1:6])
    w_hbm = bundle(WEIGHTS, refs[6:18])
    window_hbm, latent_hbm = refs[18:20]
    out = refs[20]
    s = bundle(names, refs[21:])
    small = bundle(SMALL, [getattr(s, "small_" + name) for name in SMALL])
    merged = "w_qkv" in names
    kept = [name for name in WEIGHTS if "w_" + name in names]
    w = bundle(kept, [getattr(s, "w_" + name) for name in kept])
    ownf, feat, normed = s.ownf, s.feat, s.normed
    kvb, local_kv, halo, queries, q_full, latq = s.kvb, s.local_kv, s.halo, s.queries, s.q_full, s.latq
    gates, winb, lat, top, total, acc = s.gates, s.winb, s.lat, s.top, s.total, s.acc
    wcol, columns, psend, precv = s.wcol, s.columns, s.psend, s.precv
    cosine, sine = s.cosine, s.sine

    sp, tp = lax.axis_index("sp"), lax.axis_index("tp")
    z, x = sp // n_x, lax.rem(sp, n_x)
    y, core = tp // 2, lax.rem(tp, 2)
    other = 1 - core
    sibling = y * 2 + other
    rows, block = features.shape
    half = rows // 2
    pieces = normed.shape[1]
    piece = half // pieces
    lat_heads = w_hbm.key_up.shape[1] // NOPE
    kv_width = w_hbm.key.shape[1]
    kv_heads = kv_width // HEAD
    group = w_hbm.query.shape[1] // kv_width
    latent = w_hbm.kv_latent.shape[1]
    out_parts = lat.shape[1]
    out_rows = rows // out_parts

    def remote(src, dst, send, recv, where):
        return pltpu.make_async_remote_copy(
            src_ref=src, dst_ref=dst, send_sem=send, recv_sem=recv,
            device_id=where, device_id_type=MESH,
        )

    to_sibling = {"sp": sp, "tp": sibling}

    def arrival(ref, recv):
        return remote(ref, ref, recv, recv, to_sibling)

    def start(copies):
        for copy in copies:
            copy.start()

    def own_rows(c, h):
        return ownf.at[pl.ds(pl.multiple_of(c * half + h * piece, 16), piece)]

    def feat_rows(j, h):
        return feat.at[j, pl.ds(h * piece, piece)]

    own_load = [
        pltpu.make_async_copy(features, ownf, s.own_sem.at[0]),
        pltpu.make_async_copy(
            features.at[pl.ds(pl.multiple_of(core * half, 16), half)], feat.at[tp], s.own_sem.at[1]),
    ]
    start(own_load)
    loads = bundle(SMALL, [
        pltpu.make_async_copy(getattr(small_hbm, name), getattr(small, name), s.small_sem.at[i])
        for i, name in enumerate(SMALL)
    ])
    for name in SMALL:
        getattr(loads, name).start()

    barrier = pltpu.get_barrier_semaphore()

    def greet(where):
        pl.semaphore_signal(barrier, inc=1, device_id=where, device_id_type=MESH)

    for d in range(1, n_tp):
        greet({"sp": sp, "tp": lax.rem(tp + d, n_tp)})
    for d in range(1, n_x):
        greet({"sp": z * n_x + lax.rem(x + d, n_x), "tp": tp})

    @pl.when(z + 1 < n_z)
    def _():
        greet({"sp": sp + n_x, "tp": tp})

    @pl.when(z > 0)
    def _():
        greet({"sp": sp - n_x, "tp": tp})

    @pl.when(sp + 1 < n_sp)
    def _():
        greet({"sp": sp + 1, "tp": tp})

    @pl.when(sp > 0)
    def _():
        greet({"sp": sp - 1, "tp": tp})

    one, none = jnp.int32(1), jnp.int32(0)
    pl.semaphore_wait(
        barrier,
        n_tp - 1 + n_x - 1
        + jnp.where(z + 1 < n_z, one, none) + jnp.where(z > 0, one, none)
        + jnp.where(sp + 1 < n_sp, one, none) + jnp.where(sp > 0, one, none),
    )

    def feature_sends(h):
        sends = []
        for d in range(1, n_y):
            for c in range(2):
                sends.append(remote(
                    own_rows(c, h), feat_rows(tp, h), s.f_send.at[d], s.f_recv.at[h],
                    {"sp": sp, "tp": lax.rem(y + d, n_y) * 2 + c}))
        sends.append(remote(
            own_rows(other, h), feat_rows(tp, h), s.f_send.at[0], s.f_recv.at[h], to_sibling))
        return sends

    def feature_wait(h):
        arrival(feat.at[pl.ds(0, n_tp - 1), pl.ds(h * piece, piece)], s.f_recv.at[h]).wait_recv()

    for copy in own_load:
        copy.wait()
    for h in range(pieces):
        start(feature_sends(h))

    first = 0
    for i, name in enumerate(WEIGHTS):
        source = getattr(w_hbm, name)
        if name in kept:
            to = getattr(w, name)
        else:
            to = s.w_qkv.at[:, pl.ds(first, source.shape[1])]
            first += source.shape[1]
        copy = pltpu.make_async_copy(source, to, s.w_sem.at[i])
        copy.start()
        setattr(loads, name, copy)

    def window_columns():
        local, sends = [], []
        for j in range(n_y):
            local.append(pltpu.make_async_copy(
                window_hbm.at[:, pl.ds(pl.multiple_of((j * 2 + core) * block, LANES), block)],
                wcol.at[core, j], s.w_sems.at[0]))
            sends.append(remote(
                window_hbm.at[:, pl.ds(pl.multiple_of((j * 2 + other) * block, LANES), block)],
                wcol.at[core, j], s.w_sems.at[1], s.w_sems.at[2], to_sibling))
        return local, sends

    paired = n_z % 2 == 0
    parity = lax.rem(z, 2)
    partner = {"sp": sp + n_x * (1 - 2 * parity), "tp": tp}

    def column_send(to, d):
        return remote(
            latent_hbm.at[:, pl.ds(pl.multiple_of(to * block, LANES), block)],
            columns.at[tp], s.col_send.at[d], s.col_recv.at[d], {"sp": sp, "tp": to})

    def when_across(act):
        if paired:
            pl.when(core == parity)(act)
        else:
            act()

    def column_start():
        column_send(sibling, 0).start()

        @when_across
        def _():
            for d in range(1, n_y):
                for c in range(2):
                    column_send(lax.rem(y + d, n_y) * 2 + c, d).start()

    def pair_copy(d):
        ref = columns.at[lax.rem(y + n_y - d, n_y) * 2 + parity]
        return remote(ref, ref, s.pair_send.at[d - 1], s.pair_recv.at[d - 1], partner)

    def pair_forward():
        if paired:
            for d in range(1, n_y):
                source = lax.rem(y + n_y - d, n_y) * 2 + parity
                arrival(columns.at[source], s.col_recv.at[d]).wait_recv()
                pair_copy(d).start()

    column_local = pltpu.make_async_copy(
        latent_hbm.at[:, pl.ds(pl.multiple_of(tp * block, LANES), block)],
        columns.at[tp], s.col_own.at[0])

    wcol_local, wcol_sends = window_columns()

    loads.frequency.wait()
    positions = (sp * rows + lax.broadcasted_iota(jnp.int32, (rows, ROPE), 0)).astype(F32)
    angles = positions * small.frequency[...]
    lane = lax.broadcasted_iota(jnp.int32, (rows, ROPE), 1)
    cosine[...] = jnp.cos(angles).reshape(cosine.shape)
    turned = jnp.sin(angles)
    sine[...] = jnp.where(lane < ROPE // 2, -turned, turned).reshape(sine.shape)

    def normalize(h):
        squares = jnp.zeros((piece, 1), F32)
        part = slice(h * piece, (h + 1) * piece)
        for j in range(n_tp):
            values = feat[j, part].astype(F32)
            squares = squares + jnp.sum(values * values, axis=-1, keepdims=True)
        scale = lax.rsqrt(squares / (n_tp * block) + EPS)
        for j in range(n_tp):
            span = slice(j * block, (j + 1) * block)
            values = feat[j, part].astype(F32) * scale * small.norm_gain[:, span]
            normed[core, h, :, span] = values.astype(BF16)

    def normed_copy(h):
        return remote(normed.at[core, h], normed.at[core, h], s.n_sems.at[0], s.n_sems.at[1], to_sibling)

    def latents(h):
        own = normed[core, h]
        rope = dot_t(own, w.rope[...])
        rope = rope * cosine[core, h] + swap_halves(rope) * sine[core, h]
        rope = jnp.concatenate([rope, jnp.zeros((piece, LANES - ROPE), F32)], axis=1).astype(BF16)
        kvb[sp, core, h, :, :latent] = rms_rows(dot(own, w.kv_latent[...]), small.kv_gain[...]).astype(BF16)
        kvb[sp, core, h, :, latent:] = rope

    def column_slot(k):
        return (z - k) * n_x + x

    def row_slot(k, d):
        return (z - k) * n_x + lax.rem(x + n_x - d, n_x)

    def z_copy(k, h):
        ref = kvb.at[column_slot(k), core, h]
        return remote(ref, ref, s.z_send.at[k], s.z_recv.at[h, k], {"sp": sp + n_x, "tp": tp})

    def x_copy(k, d, h):
        ref = kvb.at[column_slot(k), core, h]
        return remote(ref, ref, s.x_send.at[k, d - 1], s.x_recv.at[h, k, d - 1],
                      {"sp": z * n_x + lax.rem(x + d, n_x), "tp": tp})

    def c_copy(k, h):
        ref = kvb.at[column_slot(k), core, h]
        return remote(ref, ref, s.c_send.at[k], s.c_recv.at[k], to_sibling)

    def d_copy(k, d, h):
        ref = kvb.at[row_slot(k, d), core, h]
        return remote(ref, ref, s.d_send.at[k, d - 1], s.d_recv.at[k, d - 1], to_sibling)

    def wait_column(k):
        arrival(kvb.at[column_slot(k), other], s.c_recv.at[k]).wait_recv()

    def wait_row(k, d):
        arrival(kvb.at[row_slot(k, d), other], s.d_recv.at[k, d - 1]).wait_recv()

    def sends_row(k, d):
        return (k > 0) | (x + d < n_x)

    def takes_row(k, d):
        return (k > 0) | (x >= d)

    def pass_on(k, h):
        @pl.when(z + 1 < n_z)
        def _():
            z_copy(k, h).start()

        for d in range(1, n_x):
            @pl.when(sends_row(k, d))
            def _():
                x_copy(k, d, h).start()

        c_copy(k, h).start()

    def take_column(k, h):
        arrival(kvb.at[column_slot(k), core, h], s.z_recv.at[h, k - 1]).wait_recv()
        pass_on(k, h)

    def take_row(k, h):
        for d in range(1, n_x):
            @pl.when(takes_row(k, d))
            def _():
                arrival(kvb.at[row_slot(k, d), core, h], s.x_recv.at[h, k, d - 1]).wait_recv()
                d_copy(k, d, h).start()

    early = min(2, pieces)

    def take_first(h):
        @pl.when(z >= 1)
        def _():
            take_column(1, h)

    start(wcol_local)
    start(wcol_sends)
    column_local.start()
    for name in ("norm_gain", "kv_gain", "kv_latent", "rope"):
        getattr(loads, name).wait()
    for h in range(pieces):
        feature_wait(h)
        if h == pieces - 1:
            column_start()
        normalize(h)
        normed_copy(h).start()
        latents(h)
        pass_on(0, h)
        if h >= early:
            take_first(h - early)

    loads.query_latent.wait()
    loads.q_gain.wait()
    own_normed = normed[core].reshape(half, n_tp * block)
    latq[core] = rms_rows(dot(own_normed, w.query_latent[...]), small.q_gain[...]).astype(BF16)
    latq_copy = remote(latq.at[core], latq.at[core], s.q_sems.at[0], s.q_sems.at[1], to_sibling)
    latq_copy.start()

    for h in range(pieces - early, pieces - 1):
        take_first(h)

    arrival(normed.at[other], s.n_sems.at[1]).wait_recv()

    def all_normed():
        return normed[...].reshape(rows, n_tp * block)

    for name in MERGED:
        getattr(loads, name).wait()
    if merged:
        qkv = dot(all_normed(), s.w_qkv[...]).astype(BF16)
    else:
        qkv = jnp.concatenate([dot(all_normed(), getattr(w, name)[...]) for name in MERGED], axis=1).astype(BF16)
    local_kv[...] = qkv[:, : 2 * kv_width]
    queries[...] = qkv[:, 2 * kv_width :]
    tail = local_kv.at[pl.ds(rows - WINDOW, WINDOW)]
    halo_copy = remote(tail, halo, s.halo_sem.at[0], s.halo_sem.at[1], {"sp": sp + 1, "tp": tp})

    @pl.when(sp + 1 < n_sp)
    def _():
        halo_copy.start()

    take_first(pieces - 1)

    def queries_up():
        arrival(latq.at[other], s.q_sems.at[1]).wait_recv()
        loads.content.wait()
        loads.rotary.wait()
        latent_query = latq[...].reshape(rows, latent)
        content = dot(latent_query, w.content[...])
        rotary = dot(latent_query, w.rotary[...])
        cos_all, sin_all = cosine[...].reshape(rows, ROPE), sine[...].reshape(rows, ROPE)
        padding = jnp.zeros((rows, LANES - ROPE), F32)
        for h in range(lat_heads):
            turned = rotary[:, h * ROPE : (h + 1) * ROPE]
            turned = turned * cos_all + swap_halves(turned) * sin_all
            q_full[h, :NOPE, :] = content[:, h * NOPE : (h + 1) * NOPE].T.astype(BF16)
            q_full[h, NOPE:, :] = jnp.concatenate([turned, padding], axis=1).T.astype(BF16)
        loads.key_up.wait()
        loads.value_up.wait()

    def attend(slot, diagonal):
        both = kvb[slot].reshape(rows, latent + LANES)
        source, rope_part = both[:, :latent], both[:, latent:]
        keys = dot(source, w.key_up[...]).astype(BF16)
        values = dot(source, w.value_up[...]).astype(BF16)
        heads = range(lat_heads)
        scores = []
        for h in heads:
            key = jnp.concatenate([keys[:, h * NOPE : (h + 1) * NOPE], rope_part], axis=1)
            scores.append(dot(key, q_full[h]) * ((NOPE + ROPE) ** (-0.5) * LOG2_E))
        if diagonal:
            live = (lax.broadcasted_iota(jnp.int32, (rows, rows), 0)
                    <= lax.broadcasted_iota(jnp.int32, (rows, rows), 1))
            scores = [jnp.where(live, part, NEGATIVE) for part in scores]
        weights, fades = [], []
        for h in heads:
            peak = jnp.max(scores[h], axis=0, keepdims=True)
            if not diagonal:
                before = top[h]
                peak = jnp.maximum(peak, before)
                fades.append(jnp.exp2(before - peak))
            top[h] = peak
            weights.append(jnp.exp2(scores[h] - peak))
        for h in heads:
            weight_sum = jnp.sum(weights[h], axis=0, keepdims=True)
            part = dot_tl(values[:, h * VDIM : (h + 1) * VDIM], weights[h].astype(BF16))
            if not diagonal:
                weight_sum = total[h] * fades[h] + weight_sum
                part = acc[h] * fades[h] + part
            total[h] = weight_sum
            acc[h] = part

    def window():
        loads.sinks.wait()

        @pl.when(sp > 0)
        def _():
            arrival(halo, s.halo_sem.at[1]).wait_recv()

        @pl.when(sp == 0)
        def _():
            halo[...] = jnp.zeros(halo.shape, BF16)

        row = lax.broadcasted_iota(jnp.int32, (2 * WINDOW, WINDOW), 1)
        column = lax.broadcasted_iota(jnp.int32, (2 * WINDOW, WINDOW), 0)
        offset = row + WINDOW - column
        in_band = (offset >= 0) & (offset < WINDOW)
        in_band = jnp.concatenate([in_band] * group, axis=1)
        later = jnp.concatenate([(sp > 0) | (column >= WINDOW)] * group, axis=1)
        units = [(n, g) for n in range(rows // WINDOW) for g in range(kv_heads)]
        scores, values, sinks, weights = [], [], [], []
        for n, g in units:
            at = slice(n * WINDOW, (n + 1) * WINDOW)
            earlier = halo[...] if n == 0 else local_kv[(n - 1) * WINDOW : n * WINDOW]
            band = jnp.concatenate([earlier, local_kv[at]], axis=0)
            valid = in_band & later if n == 0 else in_band
            key = band[:, g * HEAD : (g + 1) * HEAD]
            values.append(band[:, kv_width + g * HEAD : kv_width + (g + 1) * HEAD])
            members = range(g * group, (g + 1) * group)
            query = jnp.concatenate([queries[at, q * HEAD : (q + 1) * HEAD] for q in members], axis=0)
            sinks.append(jnp.concatenate([jnp.full((1, WINDOW), small.sinks[0, q], F32) for q in members], axis=1))
            scores.append(jnp.where(valid, dot_t(key, query) * HEAD ** (-0.5), NEGATIVE))
        for u in range(len(units)):
            peak = jnp.maximum(jnp.max(scores[u], axis=0, keepdims=True), sinks[u])
            part = jnp.exp(scores[u] - peak)
            bottom = jnp.sum(part, axis=0, keepdims=True) + jnp.exp(sinks[u] - peak)
            weights.append((part * (1.0 / bottom)).astype(BF16))
        mixed = [dot_tl(values[u], weights[u]) for u in range(len(units))]
        for n in range(rows // WINDOW):
            heads = [
                mixed[n * kv_heads + g][:, i * WINDOW : (i + 1) * WINDOW]
                for g in range(kv_heads) for i in range(group)
            ]
            winb[core, n * WINDOW : (n + 1) * WINDOW, :] = jnp.concatenate(heads, axis=0).T.astype(BF16)

    win_copy = remote(winb.at[core], winb.at[core], s.win_sem.at[0], s.win_sem.at[1], to_sibling)

    def window_part(j):
        return dot(winb[0], wcol[0, j]) + dot(winb[1], wcol[1, j])

    def part_copy(d):
        return remote(psend.at[d - 1], precv.at[d - 1], s.p_send.at[d - 1], s.p_recv.at[d - 1],
                      {"sp": sp, "tp": lax.rem(y + d, n_y) * 2 + core})

    def window_parts():
        pltpu.make_async_copy(wcol.at[core], wcol.at[core], s.w_sems.at[0]).wait()
        arrival(wcol.at[other], s.w_sems.at[2]).wait_recv()
        arrival(winb.at[other], s.win_sem.at[1]).wait_recv()
        for d in range(1, n_y):
            psend[d - 1] = window_part(lax.rem(y + d, n_y)).astype(BF16)
            part_copy(d).start()

    def gate(b):
        name = WEIGHTS[10 + b]
        getattr(loads, name).wait()

        def step(i, _):
            at = pl.ds(pl.multiple_of(i * 256, LANES), 256)
            gates[b, :, at] = jax.nn.sigmoid(dot(all_normed(), getattr(w, name)[:, at]))
            return 0

        lax.fori_loop(0, block // 256, step, 0)

    def take_second(lo, hi):
        for h in range(lo, hi):
            @pl.when(z >= 2)
            def _():
                take_column(2, h)

    def take_rows(k):
        for h in range(pieces):
            take_row(k, h)

    def attend_row(k, d):
        wait_row(k, d)
        attend(row_slot(k, d), False)

    if n_z > 2:
        take_second(0, pieces // 2)
    queries_up()
    if n_z > 2:
        take_second(pieces // 2, pieces - pieces // 4)
    take_rows(0)
    wait_column(0)
    attend(sp, True)
    if n_z > 2:
        take_second(pieces - pieces // 4, pieces)
    pair_forward()

    def step(k, _):
        @pl.when(k == 3)
        def _():
            window()
            win_copy.start()

        @pl.when(z >= k - 1)
        def _():
            wait_column(k - 1)
            attend(column_slot(k - 1), False)

        @pl.when(k == 3)
        def _():
            window_parts()

        @pl.when((k > 2) & (z >= k))
        def _():
            for h in range(pieces):
                take_column(k, h)

        @pl.when(z >= k - 1)
        def _():
            take_rows(k - 1)

        for d in range(1, n_x):
            @pl.when((z >= k - 2) & takes_row(k - 2, d))
            def _():
                attend_row(k - 2, d)

        return 0

    lax.fori_loop(2, max(n_z, 2) + 2, step, 0)

    def gather(part):
        own = lat.at[tp, part]
        sends = [
            remote(own, own, s.y_send.at[d - 1], s.y_recv.at[part, d - 1],
                   {"sp": sp, "tp": lax.rem(y + d, n_y) * 2 + core})
            for d in range(1, n_y)
        ]
        sends.append(remote(own, own, s.s_send.at[0], s.s_recv.at[part], to_sibling))
        return sends

    def forward(part):
        for d in range(1, n_y):
            ref = lat.at[lax.rem(y + n_y - d, n_y) * 2 + core, part]
            arrival(ref, s.y_recv.at[part, d - 1]).wait_recv()
            remote(ref, ref, s.s_send.at[d], s.s_recv.at[part], to_sibling).start()

    def arrived(part):
        arrival(lat.at[pl.ds(0, n_y), part], s.s_recv.at[part]).wait_recv()

    for part in range(out_parts):
        at = slice(part * out_rows, (part + 1) * out_rows)
        for h in range(lat_heads):
            lat[tp, part, :, h * VDIM : (h + 1) * VDIM] = (
                acc[h, :, at] / total[h, :, at]).T.astype(BF16)
        start(gather(part))
    gate(0)
    gate(1)
    window_branch = window_part(y)
    for d in range(1, n_y):
        arrival(precv.at[d - 1], s.p_recv.at[d - 1]).wait_recv()
        window_branch = window_branch + precv[d - 1].astype(F32)
    gates[0] = gates[0] * window_branch
    column_local.wait()
    arrival(columns.at[sibling], s.col_recv.at[0]).wait_recv()
    for d in range(1, n_y):
        base = lax.rem(y + n_y - d, n_y) * 2
        if paired:
            arrival(columns.at[base + 1 - parity], s.pair_recv.at[d - 1]).wait_recv()
        else:
            arrival(columns.at[pl.ds(base, 2)], s.col_recv.at[d]).wait_recv()
    for part in range(out_parts):
        at = slice(part * out_rows, (part + 1) * out_rows)
        forward(part)
        arrived(part)
        latent_branch = jnp.zeros((out_rows, block), F32)
        for j in range(n_tp):
            latent_branch = latent_branch + dot(lat[j, part], columns[j])
        out[at, :] = (gates[0, at] + gates[1, at] * latent_branch).astype(BF16)

    def leave(ref, send):
        remote(ref, ref, send, send, to_sibling).wait_send()

    leave(ownf.at[pl.ds(0, half)], s.f_send.at[0])
    for d in range(1, n_y):
        leave(ownf, s.f_send.at[d])
    leave(normed.at[core], s.n_sems.at[0])
    latq_copy.wait_send()
    leave(wcol.at[core], s.w_sems.at[1])
    leave(columns.at[tp], s.col_send.at[0])

    @when_across
    def _():
        for d in range(1, n_y):
            leave(columns.at[pl.ds(0, 2)], s.col_send.at[d])

    if paired:
        for d in range(1, n_y):
            pair_copy(d).wait_send()
    win_copy.wait_send()
    for d in range(1, n_y):
        part_copy(d).wait_send()
        leave(lat.at[tp], s.y_send.at[d - 1])
        leave(lat.at[tp], s.s_send.at[d])
    leave(lat.at[tp], s.s_send.at[0])

    @pl.when(sp + 1 < n_sp)
    def _():
        halo_copy.wait_send()

    def drain(k, _):
        @pl.when(z >= k)
        def _():
            own = kvb.at[column_slot(k), core]

            @pl.when(z + 1 < n_z)
            def _():
                leave(own, s.z_send.at[k])

            leave(own, s.c_send.at[k])
            for d in range(1, n_x):
                @pl.when(sends_row(k, d))
                def _():
                    leave(own, s.x_send.at[k, d - 1])

                @pl.when(takes_row(k, d))
                def _():
                    leave(own, s.d_send.at[k, d - 1])

        return 0

    lax.fori_loop(0, n_z, drain, 0)


def on_device(dims, features, norm_gain, w_query, w_key, w_value, head_sinks, w_query_latent,
              w_kv_latent, w_rope_key, query_latent_gain, kv_latent_gain, w_query_content,
              w_query_rotary, w_key_up, w_value_up, w_branch_window, w_branch_latent,
              w_gate_window, w_gate_latent):
    n_sp, n_tp, n_x = dims
    n_z, n_y = n_sp // n_x, n_tp // 2
    rows, block = features.shape
    width = norm_gain.shape[0]
    latent = w_kv_latent.shape[1]
    lat_heads = w_key_up.shape[1] // NOPE
    half_width = ROPE // 2
    entry = np.arange(ROPE, dtype=np.int32) % half_width
    frequency = (np.float32(THETA) ** (-entry.astype(np.float32) / np.float32(half_width))).astype(np.float32)[None, :]
    weights = (w_kv_latent, w_rope_key.T, w_key, w_value, w_query, w_query_latent, w_query_content,
               w_query_rotary, w_key_up, w_value_up, w_gate_window, w_gate_latent)
    smalls = (norm_gain[None, :], head_sinks[None, :], query_latent_gain[None, :], kv_latent_gain[None, :],
              jnp.asarray(frequency))
    branch_rows = w_branch_window.shape[0]
    pieces = PIECES if (rows // 2) % (16 * PIECES) == 0 else 1
    piece = rows // 2 // pieces
    out_parts = rows // LANES
    merge = w_key.shape[1] % LANES == 0
    hbm = pl.BlockSpec(memory_space=pl.ANY)
    dma = pltpu.SemaphoreType.DMA
    vm = pltpu.VMEM
    scratch = dict(
        **{"small_" + n: (pltpu.SMEM if n == "sinks" else vm)(a.shape, F32) for n, a in zip(SMALL, smalls)},
        **{"w_" + n: vm(a.shape, BF16) for n, a in zip(WEIGHTS, weights) if not (merge and n in MERGED)},
        **(dict(w_qkv=vm((width, 2 * w_key.shape[1] + w_query.shape[1]), BF16)) if merge else {}),
        ownf=vm((rows, block), BF16),
        feat=vm((n_tp, rows // 2, block), BF16),
        normed=vm((2, pieces, piece, width), BF16),
        latq=vm((2, rows // 2, latent), BF16),
        wcol=vm((2, n_y, branch_rows, block), BF16),
        columns=vm((n_tp, w_branch_latent.shape[0], block), BF16),
        psend=vm((n_y - 1, rows, block), BF16),
        precv=vm((n_y - 1, rows, block), BF16),
        kvb=vm((n_sp, 2, pieces, piece, latent + LANES), BF16),
        local_kv=vm((rows, 2 * w_key.shape[1]), BF16),
        halo=vm((WINDOW, 2 * w_key.shape[1]), BF16),
        queries=vm((rows, w_query.shape[1]), BF16),
        q_full=vm((lat_heads, NOPE + LANES, rows), BF16),
        gates=vm((2, rows, block), F32),
        winb=vm((2, rows, w_query.shape[1]), BF16),
        lat=vm((n_tp, out_parts, rows // out_parts, lat_heads * VDIM), BF16),
        top=vm((lat_heads, 1, rows), F32),
        total=vm((lat_heads, 1, rows), F32),
        acc=vm((lat_heads, VDIM, rows), F32),
        cosine=vm((2, pieces, piece, ROPE), F32),
        sine=vm((2, pieces, piece, ROPE), F32),
        own_sem=dma((2,)),
        small_sem=dma((len(SMALL),)),
        w_sem=dma((len(weights),)),
        f_send=dma((n_y,)),
        f_recv=dma((pieces,)),
        n_sems=dma((2,)),
        q_sems=dma((2,)),
        w_sems=dma((3,)),
        col_own=dma((1,)),
        col_send=dma((n_y,)),
        col_recv=dma((n_y,)),
        pair_send=dma((n_y - 1,)),
        pair_recv=dma((n_y - 1,)),
        halo_sem=dma((2,)),
        win_sem=dma((2,)),
        p_send=dma((n_y - 1,)),
        p_recv=dma((n_y - 1,)),
        y_send=dma((n_y - 1,)),
        y_recv=dma((out_parts, n_y - 1)),
        s_send=dma((n_y,)),
        s_recv=dma((out_parts,)),
        z_send=dma((n_z - 1,)),
        z_recv=dma((pieces, n_z - 1)),
        x_send=dma((n_z, n_x - 1)),
        x_recv=dma((pieces, n_z, n_x - 1)),
        c_send=dma((n_z,)),
        c_recv=dma((n_z,)),
        d_send=dma((n_z, n_x - 1)),
        d_recv=dma((n_z, n_x - 1)),
    )
    return pl.pallas_call(
        functools.partial(kernel, dims, tuple(scratch)),
        out_shape=pltpu.VMEM((rows, block), BF16),
        in_specs=[hbm] * (1 + len(smalls) + len(weights) + 2),
        out_specs=pl.BlockSpec(memory_space=pltpu.VMEM),
        scratch_shapes=list(scratch.values()),
        compiler_params=pltpu.CompilerParams(
            collective_id=0, has_side_effects=True, vmem_limit_bytes=60 * 1024 * 1024
        ),
    )(features, *smalls, *weights, w_branch_window, w_branch_latent)


def solution(mesh):
    n_sp, n_tp = mesh.shape["sp"], mesh.shape["tp"]
    n_x = 1
    while n_sp % (2 * n_x) == 0 and 8 * n_x * n_x <= n_sp:
        n_x *= 2
    return jax.shard_map(
        functools.partial(on_device, (n_sp, n_tp, n_x)),
        mesh=mesh,
        in_specs=(
            P("sp", "tp"),
            P(),
            P(None, "tp"),
            P(None, "tp"),
            P(None, "tp"),
            P("tp"),
            P(),
            P(),
            P(),
            P(),
            P(),
            P(None, "tp"),
            P(None, "tp"),
            P(None, "tp"),
            P(None, "tp"),
            P("tp", None),
            P("tp", None),
            P(None, "tp"),
            P(None, "tp"),
        ),
        out_specs=P("sp", "tp"),
        check_vma=False,
    )
```

time: 60.3 us -> 46.6 us (0.77)
  Pallas kernels: 57.7 us -> 45.7 us
  local copies, waits for them, and re-layouts: 1.77 us -> 0.75 us
    pallas_call x1, Pallas kernels: 57.7 us -> 45.7 us  [on_device(): pl.pallas_call(functools.partial(kernel, dims, tuple(scratch)), out_shape...]
    unnamed x1, local copies, waits for them, and re-layouts: 1.77 us -> 0.75 us
where the time goes in v1:
time: 46.6 us; the launch traced here: 46.5 us
  Pallas kernels  45.7 us (98%)
  local copies, waits for them, and re-layouts  0.75 us (2%)
    pallas_call x1, Pallas kernels, on_device(): pl.pallas_call(functools.partial(kernel, dims, tuple(scratch)), out_shape...  45.7 us

profile of v1, /device:TPU:25, one launch (start us, length us, event | category | flops | bytes accessed | tf_op | source)
XLA Modules:
  0.0 46.5 jit_solution(847312142450002271)
XLA Ops:
  0.0 45.7 %shard_map.190 = bf16[384,512]{1,0:T(8,128)(2,1)S(1)} custom-call(bf16[384,512]{1,0:T(8,128)(2,1)} %refs_0_.1, f32[1,2048]{1,0:T(1,128)} %bitcast.6, f32[1,4]{1,0:T(1,128)} %bitcast.9, f32[1,512]{1,0:T(1,128)} %bitcast.7, f32[1,512]{1,0:T(1,128)} %bitcast.8, f32[1,64]{1,0:T(1,128)} %constant.2.clone.refs_5_, bf16[2048,512]{1,0:T(8,128)(2,1)} %refs_6_.1, ...), custom_call_target="tpu_custom_call" | custom-call | tf_op jit(solution)/shard_map/pallas_call | solution.py:756
  45.7 0.7 %copy.22 = bf16[384,512]{1,0:T(8,128)(2,1)} copy(bf16[384,512]{1,0:T(8,128)(2,1)S(1)} %shard_map.190) | data formatting | bytes 786432

commit v2 on v1

--- a/solution.py
+++ b/solution.py
@@ -25,6 +25,8 @@
 BF16 = jnp.bfloat16
 F32 = jnp.float32
 PIECES = 4
+SUBLANES = 8
+DETOURS = (0, PIECES - 1)
 
 
 def dot(left, right):
@@ -274,9 +276,21 @@
         own = normed[core, h]
         rope = dot_t(own, w.rope[...])
         rope = rope * cosine[core, h] + swap_halves(rope) * sine[core, h]
-        rope = jnp.concatenate([rope, jnp.zeros((piece, LANES - ROPE), F32)], axis=1).astype(BF16)
-        kvb[sp, core, h, :, :latent] = rms_rows(dot(own, w.kv_latent[...]), small.kv_gain[...]).astype(BF16)
-        kvb[sp, core, h, :, latent:] = rope
+        rope = jnp.concatenate([rope[: piece // 2], rope[piece // 2 :]], axis=1)
+        rope = [rope[i : i + SUBLANES] for i in range(0, piece // 2, SUBLANES)]
+        rope.append(jnp.zeros((SUBLANES, latent - len(rope) * LANES), F32))
+        kvb[sp, core, h, :piece, :] = rms_rows(dot(own, w.kv_latent[...]), small.kv_gain[...]).astype(BF16)
+        kvb[sp, core, h, piece:, :] = jnp.concatenate(rope, axis=1).astype(BF16)
+
+    def rope_rows(slot):
+        parts = []
+        for c in range(2):
+            for h in range(pieces):
+                packed = kvb[slot, c, h, piece:, :].astype(F32)
+                pair = jnp.concatenate(
+                    [packed[:, i * LANES : (i + 1) * LANES] for i in range(piece // 2 // SUBLANES)], axis=0)
+                parts += [pair, pltpu.roll(pair, ROPE, 1)]
+        return jnp.concatenate(parts, axis=0).astype(BF16)
 
     def column_slot(k):
         return (z - k) * n_x + x
@@ -313,13 +327,20 @@
     def takes_row(k, d):
         return (k > 0) | (x >= d)
 
+    def detoured(k, h, to):
+        if h == DETOURS[0]:
+            return k >= 2
+        return (k >= 3) & (to == 0)
+
     def pass_on(k, h):
         @pl.when(z + 1 < n_z)
         def _():
             z_copy(k, h).start()
 
         for d in range(1, n_x):
-            @pl.when(sends_row(k, d))
+            to = lax.rem(x + d, n_x)
+
+            @pl.when(sends_row(k, d) & ~detoured(k, h, to) if h in DETOURS else sends_row(k, d))
             def _():
                 x_copy(k, d, h).start()
 
@@ -329,11 +350,32 @@
         arrival(kvb.at[column_slot(k), core, h], s.z_recv.at[h, k - 1]).wait_recv()
         pass_on(k, h)
 
+    def detour_copy(k, d, i):
+        ref = kvb.at[row_slot(k, d), core, DETOURS[i]]
+        return remote(ref, ref, s.r_send.at[i, k, d - 1], s.r_recv.at[i, k + 1, d - 1], {"sp": sp + n_x, "tp": tp})
+
+    def passes_detour(k, i):
+        return (z + 1 < n_z) & detoured(k + 1, DETOURS[i], x)
+
     def take_row(k, h):
         for d in range(1, n_x):
+            def from_x():
+                arrival(kvb.at[row_slot(k, d), core, h], s.x_recv.at[h, k, d - 1]).wait_recv()
+
+            def from_z():
+                arrival(kvb.at[row_slot(k, d), core, h], s.r_recv.at[DETOURS.index(h), k, d - 1]).wait_recv()
+
             @pl.when(takes_row(k, d))
             def _():
-                arrival(kvb.at[row_slot(k, d), core, h], s.x_recv.at[h, k, d - 1]).wait_recv()
+                if h in DETOURS:
+                    pl.when(~detoured(k, h, x))(from_x)
+                    pl.when(detoured(k, h, x))(from_z)
+
+                    @pl.when(passes_detour(k, DETOURS.index(h)))
+                    def _():
+                        detour_copy(k, d, DETOURS.index(h)).start()
+                else:
+                    from_x()
                 d_copy(k, d, h).start()
 
     early = min(2, pieces)
@@ -366,9 +408,6 @@
     latq_copy = remote(latq.at[core], latq.at[core], s.q_sems.at[0], s.q_sems.at[1], to_sibling)
     latq_copy.start()
 
-    for h in range(pieces - early, pieces - 1):
-        take_first(h)
-
     arrival(normed.at[other], s.n_sems.at[1]).wait_recv()
 
     def all_normed():
@@ -385,11 +424,7 @@
     tail = local_kv.at[pl.ds(rows - WINDOW, WINDOW)]
     halo_copy = remote(tail, halo, s.halo_sem.at[0], s.halo_sem.at[1], {"sp": sp + 1, "tp": tp})
 
-    @pl.when(sp + 1 < n_sp)
-    def _():
-        halo_copy.start()
-
-    take_first(pieces - 1)
+    take_first(pieces - 2)
 
     def queries_up():
         arrival(latq.at[other], s.q_sems.at[1]).wait_recv()
@@ -409,8 +444,8 @@
         loads.value_up.wait()
 
     def attend(slot, diagonal):
-        both = kvb[slot].reshape(rows, latent + LANES)
-        source, rope_part = both[:, :latent], both[:, latent:]
+        source = kvb[slot, :, :, :piece, :].reshape(rows, latent)
+        rope_part = rope_rows(slot)
         keys = dot(source, w.key_up[...]).astype(BF16)
         values = dot(source, w.value_up[...]).astype(BF16)
         heads = range(lat_heads)
@@ -440,9 +475,7 @@
             total[h] = weight_sum
             acc[h] = part
 
-    def window():
-        loads.sinks.wait()
-
+    def take_halo():
         @pl.when(sp > 0)
         def _():
             arrival(halo, s.halo_sem.at[1]).wait_recv()
@@ -451,13 +484,14 @@
         def _():
             halo[...] = jnp.zeros(halo.shape, BF16)
 
+    def window(blocks):
         row = lax.broadcasted_iota(jnp.int32, (2 * WINDOW, WINDOW), 1)
         column = lax.broadcasted_iota(jnp.int32, (2 * WINDOW, WINDOW), 0)
         offset = row + WINDOW - column
         in_band = (offset >= 0) & (offset < WINDOW)
         in_band = jnp.concatenate([in_band] * group, axis=1)
         later = jnp.concatenate([(sp > 0) | (column >= WINDOW)] * group, axis=1)
-        units = [(n, g) for n in range(rows // WINDOW) for g in range(kv_heads)]
+        units = [(n, g) for n in blocks for g in range(kv_heads)]
         scores, values, sinks, weights = [], [], [], []
         for n, g in units:
             at = slice(n * WINDOW, (n + 1) * WINDOW)
@@ -476,29 +510,32 @@
             bottom = jnp.sum(part, axis=0, keepdims=True) + jnp.exp(sinks[u] - peak)
             weights.append((part * (1.0 / bottom)).astype(BF16))
         mixed = [dot_tl(values[u], weights[u]) for u in range(len(units))]
-        for n in range(rows // WINDOW):
+        for b, n in enumerate(blocks):
             heads = [
-                mixed[n * kv_heads + g][:, i * WINDOW : (i + 1) * WINDOW]
+                mixed[b * kv_heads + g][:, i * WINDOW : (i + 1) * WINDOW]
                 for g in range(kv_heads) for i in range(group)
             ]
             winb[core, n * WINDOW : (n + 1) * WINDOW, :] = jnp.concatenate(heads, axis=0).T.astype(BF16)
 
-    win_copy = remote(winb.at[core], winb.at[core], s.win_sem.at[0], s.win_sem.at[1], to_sibling)
-
-    def window_part(j):
-        return dot(winb[0], wcol[0, j]) + dot(winb[1], wcol[1, j])
-
-    def part_copy(d):
-        return remote(psend.at[d - 1], precv.at[d - 1], s.p_send.at[d - 1], s.p_recv.at[d - 1],
+    def win_copy(i):
+        ref = winb.at[core, win_rows[i]]
+        return remote(ref, ref, s.win_send.at[i], s.win_recv.at[i], to_sibling)
+
+    win_rows = (pl.ds(WINDOW, rows - WINDOW), pl.ds(0, WINDOW))
+
+    def window_part(j, at):
+        return dot(winb[0, at], wcol[0, j]) + dot(winb[1, at], wcol[1, j])
+
+    def part_copy(d, at):
+        return remote(psend.at[d - 1, at], precv.at[d - 1, at], s.p_send.at[d - 1], s.p_recv.at[d - 1],
                       {"sp": sp, "tp": lax.rem(y + d, n_y) * 2 + core})
 
-    def window_parts():
-        pltpu.make_async_copy(wcol.at[core], wcol.at[core], s.w_sems.at[0]).wait()
-        arrival(wcol.at[other], s.w_sems.at[2]).wait_recv()
-        arrival(winb.at[other], s.win_sem.at[1]).wait_recv()
+    def window_parts(i):
+        at = win_rows[i]
+        arrival(winb.at[other, at], s.win_recv.at[i]).wait_recv()
         for d in range(1, n_y):
-            psend[d - 1] = window_part(lax.rem(y + d, n_y)).astype(BF16)
-            part_copy(d).start()
+            psend[d - 1, at] = window_part(lax.rem(y + d, n_y), at).astype(BF16)
+            part_copy(d, at).start()
 
     def gate(b):
         name = WEIGHTS[10 + b]
@@ -525,39 +562,68 @@
         wait_row(k, d)
         attend(row_slot(k, d), False)
 
+    loads.sinks.wait()
+    window(range(1, rows // WINDOW))
+    win_copy(0).start()
+    take_first(pieces - 1)
+    queries_up()
     if n_z > 2:
         take_second(0, pieces // 2)
-    queries_up()
-    if n_z > 2:
-        take_second(pieces // 2, pieces - pieces // 4)
+    pltpu.make_async_copy(wcol.at[core], wcol.at[core], s.w_sems.at[0]).wait()
+    arrival(wcol.at[other], s.w_sems.at[2]).wait_recv()
+    window_parts(0)
     take_rows(0)
     wait_column(0)
     attend(sp, True)
     if n_z > 2:
-        take_second(pieces - pieces // 4, pieces)
-    pair_forward()
+        take_second(pieces // 2, pieces - 1)
+
+    @pl.when(sp + 1 < n_sp)
+    def _():
+        halo_copy.start()
+
+    def take_pieces(k, lo, hi):
+        @pl.when(z >= k)
+        def _():
+            for h in range(lo, hi):
+                take_column(k, h)
+
+    near = (x > 0) | (z == 0)
+
+    def first_window():
+        take_halo()
+        window(range(1))
+        win_copy(1).start()
+
+    def last_parts():
+        window_parts(1)
 
     def step(k, _):
-        @pl.when(k == 3)
-        def _():
-            window()
-            win_copy.start()
+        @pl.when((k == 3) & (parity == 1))
+        def _():
+            pair_forward()
 
         @pl.when(z >= k - 1)
         def _():
             wait_column(k - 1)
             attend(column_slot(k - 1), False)
 
-        @pl.when(k == 3)
-        def _():
-            window_parts()
-
-        @pl.when((k > 2) & (z >= k))
-        def _():
-            for h in range(pieces):
-                take_column(k, h)
-
-        @pl.when(z >= k - 1)
+        @pl.when(k == 2)
+        def _():
+            take_pieces(k, pieces - 1, pieces)
+
+        pl.when((k == 4) & near)(last_parts)
+        pl.when((k == 4) & ~near)(first_window)
+
+        @pl.when((k == 4) & (z == 0))
+        def _():
+            pair_forward()
+
+        @pl.when(k > 2)
+        def _():
+            take_pieces(k, 0, pieces // 2)
+
+        @pl.when((z >= k - 1) & (k == n_z) & near)
         def _():
             take_rows(k - 1)
 
@@ -566,9 +632,25 @@
             def _():
                 attend_row(k - 2, d)
 
+
+        @pl.when(k > 2)
+        def _():
+            take_pieces(k, pieces // 2, pieces)
+
+        pl.when((k == 3) & near)(first_window)
+        pl.when((k == 4) & ~near)(last_parts)
+
+        @pl.when((z >= k - 1) & ~((k == n_z) & near))
+        def _():
+            take_rows(k - 1)
+
         return 0
 
-    lax.fori_loop(2, max(n_z, 2) + 2, step, 0)
+    lax.fori_loop(2, max(n_z, 3) + 2, step, 0)
+
+    @pl.when((parity == 0) & (z > 0))
+    def _():
+        pair_forward()
 
     def gather(part):
         own = lat.at[tp, part]
@@ -597,7 +679,7 @@
         start(gather(part))
     gate(0)
     gate(1)
-    window_branch = window_part(y)
+    window_branch = window_part(y, pl.ds(0, rows))
     for d in range(1, n_y):
         arrival(precv.at[d - 1], s.p_recv.at[d - 1]).wait_recv()
         window_branch = window_branch + precv[d - 1].astype(F32)
@@ -638,9 +720,10 @@
     if paired:
         for d in range(1, n_y):
             pair_copy(d).wait_send()
-    win_copy.wait_send()
+    for i in range(2):
+        win_copy(i).wait_send()
     for d in range(1, n_y):
-        part_copy(d).wait_send()
+        leave(psend.at[d - 1], s.p_send.at[d - 1])
         leave(lat.at[tp], s.y_send.at[d - 1])
         leave(lat.at[tp], s.s_send.at[d])
     leave(lat.at[tp], s.s_send.at[0])
@@ -660,9 +743,25 @@
 
             leave(own, s.c_send.at[k])
             for d in range(1, n_x):
-                @pl.when(sends_row(k, d))
+                to = lax.rem(x + d, n_x)
+                fewer = [detoured(k, h, to) for h in DETOURS]
+
+                @pl.when(sends_row(k, d) & ~fewer[0])
                 def _():
                     leave(own, s.x_send.at[k, d - 1])
+
+                @pl.when(fewer[0] & ~fewer[1])
+                def _():
+                    leave(own.at[pl.ds(0, pieces - 1)], s.x_send.at[k, d - 1])
+
+                @pl.when(fewer[1])
+                def _():
+                    leave(own.at[pl.ds(0, pieces - 2)], s.x_send.at[k, d - 1])
+
+                for i in range(2):
+                    @pl.when(takes_row(k, d) & passes_detour(k, i))
+                    def _():
+                        detour_copy(k, d, i).wait_send()
 
                 @pl.when(takes_row(k, d))
                 def _():
@@ -691,7 +790,7 @@
     smalls = (norm_gain[None, :], head_sinks[None, :], query_latent_gain[None, :], kv_latent_gain[None, :],
               jnp.asarray(frequency))
     branch_rows = w_branch_window.shape[0]
-    pieces = PIECES if (rows // 2) % (16 * PIECES) == 0 else 1
+    pieces = PIECES
     piece = rows // 2 // pieces
     out_parts = rows // LANES
     merge = w_key.shape[1] % LANES == 0
@@ -710,7 +809,7 @@
         columns=vm((n_tp, w_branch_latent.shape[0], block), BF16),
         psend=vm((n_y - 1, rows, block), BF16),
         precv=vm((n_y - 1, rows, block), BF16),
-        kvb=vm((n_sp, 2, pieces, piece, latent + LANES), BF16),
+        kvb=vm((n_sp, 2, pieces, piece + SUBLANES, latent), BF16),
         local_kv=vm((rows, 2 * w_key.shape[1]), BF16),
         halo=vm((WINDOW, 2 * w_key.shape[1]), BF16),
         queries=vm((rows, w_query.shape[1]), BF16),
@@ -737,7 +836,8 @@
         pair_send=dma((n_y - 1,)),
         pair_recv=dma((n_y - 1,)),
         halo_sem=dma((2,)),
-        win_sem=dma((2,)),
+        win_send=dma((2,)),
+        win_recv=dma((2,)),
         p_send=dma((n_y - 1,)),
         p_recv=dma((n_y - 1,)),
         y_send=dma((n_y - 1,)),
@@ -746,6 +846,8 @@
         s_recv=dma((out_parts,)),
         z_send=dma((n_z - 1,)),
         z_recv=dma((pieces, n_z - 1)),
+        r_send=dma((2, n_z, n_x - 1)),
+        r_recv=dma((2, n_z, n_x - 1)),
         x_send=dma((n_z, n_x - 1)),
         x_recv=dma((pieces, n_z, n_x - 1)),
         c_send=dma((n_z,)),

time: 46.6 us -> 42.3 us (0.908)
  Pallas kernels: 45.7 us -> 41.4 us
    pallas_call x1, Pallas kernels: 45.7 us -> 41.4 us  [on_device(): pl.pallas_call(functools.partial(kernel, dims, tuple(scratch)), out_shape...]
where the time goes in v2:
time: 42.3 us; the launch traced here: 42.1 us
  Pallas kernels  41.4 us (98%)
  local copies, waits for them, and re-layouts  0.75 us (2%)
    pallas_call x1, Pallas kernels, on_device(): pl.pallas_call(functools.partial(kernel, dims, tuple(scratch)), out_shape...  41.4 us

profile of v2, /device:TPU:25, one launch (start us, length us, event | category | flops | bytes accessed | tf_op | source)
XLA Modules:
  0.0 42.1 jit_solution(12193930658570964374)
XLA Ops:
  0.0 41.4 %shard_map.190 = bf16[384,512]{1,0:T(8,128)(2,1)S(1)} custom-call(bf16[384,512]{1,0:T(8,128)(2,1)} %refs_0_.1, f32[1,2048]{1,0:T(1,128)} %bitcast.6, f32[1,4]{1,0:T(1,128)} %bitcast.9, f32[1,512]{1,0:T(1,128)} %bitcast.7, f32[1,512]{1,0:T(1,128)} %bitcast.8, f32[1,64]{1,0:T(1,128)} %constant.2.clone.refs_5_, bf16[2048,512]{1,0:T(8,128)(2,1)} %refs_6_.1, ...), custom_call_target="tpu_custom_call" | custom-call | tf_op jit(solution)/shard_map/pallas_call | solution.py:858
  41.4 0.7 %copy.22 = bf16[384,512]{1,0:T(8,128)(2,1)} copy(bf16[384,512]{1,0:T(8,128)(2,1)S(1)} %shard_map.190) | data formatting | bytes 786432

commit v3 on v2

--- a/solution.py
+++ b/solution.py
@@ -76,6 +76,7 @@
     kept = [name for name in WEIGHTS if "w_" + name in names]
     w = bundle(kept, [getattr(s, "w_" + name) for name in kept])
     ownf, feat, normed = s.ownf, s.feat, s.normed
+    turn = s.turn
     kvb, local_kv, halo, queries, q_full, latq = s.kvb, s.local_kv, s.halo, s.queries, s.q_full, s.latq
     gates, winb, lat, top, total, acc = s.gates, s.winb, s.lat, s.top, s.total, s.acc
     wcol, columns, psend, precv = s.wcol, s.columns, s.psend, s.precv
@@ -329,7 +330,7 @@
 
     def detoured(k, h, to):
         if h == DETOURS[0]:
-            return k >= 2
+            return (k >= 2) & (to > 0)
         return (k >= 3) & (to == 0)
 
     def pass_on(k, h):
@@ -352,7 +353,7 @@
 
     def detour_copy(k, d, i):
         ref = kvb.at[row_slot(k, d), core, DETOURS[i]]
-        return remote(ref, ref, s.r_send.at[i, k, d - 1], s.r_recv.at[i, k + 1, d - 1], {"sp": sp + n_x, "tp": tp})
+        return remote(ref, ref, s.r_send.at[i, k - 1, d - 1], s.r_recv.at[i, k - 1, d - 1], {"sp": sp + n_x, "tp": tp})
 
     def passes_detour(k, i):
         return (z + 1 < n_z) & detoured(k + 1, DETOURS[i], x)
@@ -363,7 +364,7 @@
                 arrival(kvb.at[row_slot(k, d), core, h], s.x_recv.at[h, k, d - 1]).wait_recv()
 
             def from_z():
-                arrival(kvb.at[row_slot(k, d), core, h], s.r_recv.at[DETOURS.index(h), k, d - 1]).wait_recv()
+                arrival(kvb.at[row_slot(k, d), core, h], s.r_recv.at[DETOURS.index(h), k - 2, d - 1]).wait_recv()
 
             @pl.when(takes_row(k, d))
             def _():
@@ -378,7 +379,11 @@
                     from_x()
                 d_copy(k, d, h).start()
 
-    early = min(2, pieces)
+    def take_second(lo, hi):
+        for h in range(lo, hi):
+            @pl.when(z >= 2)
+            def _():
+                take_column(2, h)
 
     def take_first(h):
         @pl.when(z >= 1)
@@ -398,8 +403,8 @@
         normed_copy(h).start()
         latents(h)
         pass_on(0, h)
-        if h >= early:
-            take_first(h - early)
+        if 1 <= h <= pieces // 2:
+            take_first(h - 1)
 
     loads.query_latent.wait()
     loads.q_gain.wait()
@@ -409,6 +414,9 @@
     latq_copy.start()
 
     arrival(normed.at[other], s.n_sems.at[1]).wait_recv()
+
+    if n_z > 2:
+        take_second(0, 1)
 
     def all_normed():
         return normed[...].reshape(rows, n_tp * block)
@@ -423,6 +431,12 @@
     queries[...] = qkv[:, 2 * kv_width :]
     tail = local_kv.at[pl.ds(rows - WINDOW, WINDOW)]
     halo_copy = remote(tail, halo, s.halo_sem.at[0], s.halo_sem.at[1], {"sp": sp + 1, "tp": tp})
+    turn_copy = remote(tail, turn, s.halo_sem.at[0], s.halo_sem.at[2], {"sp": z * n_x, "tp": tp})
+    relay_copy = remote(turn, halo, s.halo_sem.at[3], s.halo_sem.at[1], {"sp": sp + n_x, "tp": tp})
+
+    @pl.when((x + 1 == n_x) & (z + 1 < n_z))
+    def _():
+        turn_copy.start()
 
     take_first(pieces - 2)
 
@@ -548,12 +562,6 @@
 
         lax.fori_loop(0, block // 256, step, 0)
 
-    def take_second(lo, hi):
-        for h in range(lo, hi):
-            @pl.when(z >= 2)
-            def _():
-                take_column(2, h)
-
     def take_rows(k):
         for h in range(pieces):
             take_row(k, h)
@@ -568,7 +576,7 @@
     take_first(pieces - 1)
     queries_up()
     if n_z > 2:
-        take_second(0, pieces // 2)
+        take_second(1, pieces // 2)
     pltpu.make_async_copy(wcol.at[core], wcol.at[core], s.w_sems.at[0]).wait()
     arrival(wcol.at[other], s.w_sems.at[2]).wait_recv()
     window_parts(0)
@@ -578,9 +586,10 @@
     if n_z > 2:
         take_second(pieces // 2, pieces - 1)
 
-    @pl.when(sp + 1 < n_sp)
+    @pl.when(x + 1 < n_x)
     def _():
         halo_copy.start()
+
 
     def take_pieces(k, lo, hi):
         @pl.when(z >= k)
@@ -599,7 +608,7 @@
         window_parts(1)
 
     def step(k, _):
-        @pl.when((k == 3) & (parity == 1))
+        @pl.when(k == 4 - parity)
         def _():
             pair_forward()
 
@@ -612,20 +621,24 @@
         def _():
             take_pieces(k, pieces - 1, pieces)
 
+            @pl.when((x == 0) & (z + 1 < n_z))
+            def _():
+                arrival(turn, s.halo_sem.at[2]).wait_recv()
+                relay_copy.start()
+
         pl.when((k == 4) & near)(last_parts)
         pl.when((k == 4) & ~near)(first_window)
 
-        @pl.when((k == 4) & (z == 0))
-        def _():
-            pair_forward()
-
         @pl.when(k > 2)
         def _():
-            take_pieces(k, 0, pieces // 2)
-
-        @pl.when((z >= k - 1) & (k == n_z) & near)
+            pl.when(x == 0)(functools.partial(take_pieces, k, 0, 1))
+            take_pieces(k, 1, pieces // 2)
+
+        @pl.when((z >= k - 1) & (k == n_z))
         def _():
             take_rows(k - 1)
+
+        pl.when((k == 4) & ~near)(last_parts)
 
         for d in range(1, n_x):
             @pl.when((z >= k - 2) & takes_row(k - 2, d))
@@ -635,22 +648,27 @@
 
         @pl.when(k > 2)
         def _():
-            take_pieces(k, pieces // 2, pieces)
+            take_pieces(k, pieces // 2, pieces - 1)
 
         pl.when((k == 3) & near)(first_window)
-        pl.when((k == 4) & ~near)(last_parts)
-
-        @pl.when((z >= k - 1) & ~((k == n_z) & near))
+
+        @pl.when(k > 2)
+        def _():
+            take_pieces(k, pieces - 1, pieces)
+
+
+        @pl.when((z >= k - 1) & (k != n_z))
         def _():
             take_rows(k - 1)
 
+        @pl.when(x > 0)
+        def _():
+            take_pieces(k + 1, 0, 1)
+
         return 0
 
     lax.fori_loop(2, max(n_z, 3) + 2, step, 0)
 
-    @pl.when((parity == 0) & (z > 0))
-    def _():
-        pair_forward()
 
     def gather(part):
         own = lat.at[tp, part]
@@ -728,9 +746,13 @@
         leave(lat.at[tp], s.s_send.at[d])
     leave(lat.at[tp], s.s_send.at[0])
 
-    @pl.when(sp + 1 < n_sp)
+    @pl.when((x + 1 < n_x) | (z + 1 < n_z))
     def _():
         halo_copy.wait_send()
+
+    @pl.when((x == 0) & (z + 1 < n_z))
+    def _():
+        relay_copy.wait_send()
 
     def drain(k, _):
         @pl.when(z >= k)
@@ -746,17 +768,13 @@
                 to = lax.rem(x + d, n_x)
                 fewer = [detoured(k, h, to) for h in DETOURS]
 
-                @pl.when(sends_row(k, d) & ~fewer[0])
+                @pl.when(sends_row(k, d) & ~(fewer[0] | fewer[1]))
                 def _():
                     leave(own, s.x_send.at[k, d - 1])
 
-                @pl.when(fewer[0] & ~fewer[1])
+                @pl.when(fewer[0] | fewer[1])
                 def _():
                     leave(own.at[pl.ds(0, pieces - 1)], s.x_send.at[k, d - 1])
-
-                @pl.when(fewer[1])
-                def _():
-                    leave(own.at[pl.ds(0, pieces - 2)], s.x_send.at[k, d - 1])
 
                 for i in range(2):
                     @pl.when(takes_row(k, d) & passes_detour(k, i))
@@ -812,6 +830,7 @@
         kvb=vm((n_sp, 2, pieces, piece + SUBLANES, latent), BF16),
         local_kv=vm((rows, 2 * w_key.shape[1]), BF16),
         halo=vm((WINDOW, 2 * w_key.shape[1]), BF16),
+        turn=vm((WINDOW, 2 * w_key.shape[1]), BF16),
         queries=vm((rows, w_query.shape[1]), BF16),
         q_full=vm((lat_heads, NOPE + LANES, rows), BF16),
         gates=vm((2, rows, block), F32),
@@ -835,7 +854,7 @@
         col_recv=dma((n_y,)),
         pair_send=dma((n_y - 1,)),
         pair_recv=dma((n_y - 1,)),
-        halo_sem=dma((2,)),
+        halo_sem=dma((4,)),
         win_send=dma((2,)),
         win_recv=dma((2,)),
         p_send=dma((n_y - 1,)),
@@ -846,8 +865,8 @@
         s_recv=dma((out_parts,)),
         z_send=dma((n_z - 1,)),
         z_recv=dma((pieces, n_z - 1)),
-        r_send=dma((2, n_z, n_x - 1)),
-        r_recv=dma((2, n_z, n_x - 1)),
+        r_send=dma((2, n_z - 2, n_x - 1)),
+        r_recv=dma((2, n_z - 2, n_x - 1)),
         x_send=dma((n_z, n_x - 1)),
         x_recv=dma((pieces, n_z, n_x - 1)),
         c_send=dma((n_z,)),

time: 42.3 us -> 41.1 us (0.972)
  Pallas kernels: 41.4 us -> 40.2 us
    pallas_call x1, Pallas kernels: 41.4 us -> 40.2 us  [on_device(): pl.pallas_call(functools.partial(kernel, dims, tuple(scratch)), out_shape...]
where the time goes in v3:
time: 41.1 us; the launch traced here: 40.9 us
  Pallas kernels  40.2 us (98%)
  local copies, waits for them, and re-layouts  0.75 us (2%)
    pallas_call x1, Pallas kernels, on_device(): pl.pallas_call(functools.partial(kernel, dims, tuple(scratch)), out_shape...  40.2 us

profile of v3, /device:TPU:25, one launch (start us, length us, event | category | flops | bytes accessed | tf_op | source)
XLA Modules:
  0.0 40.9 jit_solution(16117382563223812833)
XLA Ops:
  0.0 40.2 %shard_map.190 = bf16[384,512]{1,0:T(8,128)(2,1)S(1)} custom-call(bf16[384,512]{1,0:T(8,128)(2,1)} %refs_0_.1, f32[1,2048]{1,0:T(1,128)} %bitcast.6, f32[1,4]{1,0:T(1,128)} %bitcast.9, f32[1,512]{1,0:T(1,128)} %bitcast.7, f32[1,512]{1,0:T(1,128)} %bitcast.8, f32[1,64]{1,0:T(1,128)} %constant.2.clone.refs_5_, bf16[2048,512]{1,0:T(8,128)(2,1)} %refs_6_.1, ...), custom_call_target="tpu_custom_call" | custom-call | tf_op jit(solution)/shard_map/pallas_call | solution.py:877
  40.2 0.7 %copy.22 = bf16[384,512]{1,0:T(8,128)(2,1)} copy(bf16[384,512]{1,0:T(8,128)(2,1)S(1)} %shard_map.190) | data formatting | bytes 786432

commit v4 on v3

--- a/solution.py
+++ b/solution.py
@@ -151,20 +151,11 @@
     def _():
         greet({"sp": sp - n_x, "tp": tp})
 
-    @pl.when(sp + 1 < n_sp)
-    def _():
-        greet({"sp": sp + 1, "tp": tp})
-
-    @pl.when(sp > 0)
-    def _():
-        greet({"sp": sp - 1, "tp": tp})
-
     one, none = jnp.int32(1), jnp.int32(0)
     pl.semaphore_wait(
         barrier,
         n_tp - 1 + n_x - 1
-        + jnp.where(z + 1 < n_z, one, none) + jnp.where(z > 0, one, none)
-        + jnp.where(sp + 1 < n_sp, one, none) + jnp.where(sp > 0, one, none),
+        + jnp.where(z + 1 < n_z, one, none) + jnp.where(z > 0, one, none),
     )
 
     def feature_sends(h):
@@ -172,10 +163,10 @@
         for d in range(1, n_y):
             for c in range(2):
                 sends.append(remote(
-                    own_rows(c, h), feat_rows(tp, h), s.f_send.at[d], s.f_recv.at[h],
+                    own_rows(c, h), feat_rows(tp, h), s.sent.at[0], s.f_recv.at[h],
                     {"sp": sp, "tp": lax.rem(y + d, n_y) * 2 + c}))
         sends.append(remote(
-            own_rows(other, h), feat_rows(tp, h), s.f_send.at[0], s.f_recv.at[h], to_sibling))
+            own_rows(other, h), feat_rows(tp, h), s.sent.at[0], s.f_recv.at[h], to_sibling))
         return sends
 
     def feature_wait(h):
@@ -206,7 +197,7 @@
                 wcol.at[core, j], s.w_sems.at[0]))
             sends.append(remote(
                 window_hbm.at[:, pl.ds(pl.multiple_of((j * 2 + other) * block, LANES), block)],
-                wcol.at[core, j], s.w_sems.at[1], s.w_sems.at[2], to_sibling))
+                wcol.at[core, j], s.sent.at[0], s.w_sems.at[1], to_sibling))
         return local, sends
 
     paired = n_z % 2 == 0
@@ -216,7 +207,7 @@
     def column_send(to, d):
         return remote(
             latent_hbm.at[:, pl.ds(pl.multiple_of(to * block, LANES), block)],
-            columns.at[tp], s.col_send.at[d], s.col_recv.at[d], {"sp": sp, "tp": to})
+            columns.at[tp], s.sent.at[0], s.col_recv.at[d], {"sp": sp, "tp": to})
 
     def when_across(act):
         if paired:
@@ -235,7 +226,7 @@
 
     def pair_copy(d):
         ref = columns.at[lax.rem(y + n_y - d, n_y) * 2 + parity]
-        return remote(ref, ref, s.pair_send.at[d - 1], s.pair_recv.at[d - 1], partner)
+        return remote(ref, ref, s.sent.at[0], s.pair_recv.at[d - 1], partner)
 
     def pair_forward():
         if paired:
@@ -271,7 +262,7 @@
             normed[core, h, :, span] = values.astype(BF16)
 
     def normed_copy(h):
-        return remote(normed.at[core, h], normed.at[core, h], s.n_sems.at[0], s.n_sems.at[1], to_sibling)
+        return remote(normed.at[core, h], normed.at[core, h], s.sent.at[0], s.n_sems.at[0], to_sibling)
 
     def latents(h):
         own = normed[core, h]
@@ -283,9 +274,9 @@
         kvb[sp, core, h, :piece, :] = rms_rows(dot(own, w.kv_latent[...]), small.kv_gain[...]).astype(BF16)
         kvb[sp, core, h, piece:, :] = jnp.concatenate(rope, axis=1).astype(BF16)
 
-    def rope_rows(slot):
+    def rope_rows(slot, halves=range(2)):
         parts = []
-        for c in range(2):
+        for c in halves:
             for h in range(pieces):
                 packed = kvb[slot, c, h, piece:, :].astype(F32)
                 pair = jnp.concatenate(
@@ -301,20 +292,20 @@
 
     def z_copy(k, h):
         ref = kvb.at[column_slot(k), core, h]
-        return remote(ref, ref, s.z_send.at[k], s.z_recv.at[h, k], {"sp": sp + n_x, "tp": tp})
+        return remote(ref, ref, s.sent.at[0], s.z_recv.at[h, k], {"sp": sp + n_x, "tp": tp})
 
     def x_copy(k, d, h):
         ref = kvb.at[column_slot(k), core, h]
-        return remote(ref, ref, s.x_send.at[k, d - 1], s.x_recv.at[h, k, d - 1],
+        return remote(ref, ref, s.sent.at[0], s.x_recv.at[h, k, d - 1],
                       {"sp": z * n_x + lax.rem(x + d, n_x), "tp": tp})
 
     def c_copy(k, h):
         ref = kvb.at[column_slot(k), core, h]
-        return remote(ref, ref, s.c_send.at[k], s.c_recv.at[k], to_sibling)
+        return remote(ref, ref, s.sent.at[0], s.c_recv.at[k], to_sibling)
 
     def d_copy(k, d, h):
         ref = kvb.at[row_slot(k, d), core, h]
-        return remote(ref, ref, s.d_send.at[k, d - 1], s.d_recv.at[k, d - 1], to_sibling)
+        return remote(ref, ref, s.sent.at[0], s.d_recv.at[k, d - 1], to_sibling)
 
     def wait_column(k):
         arrival(kvb.at[column_slot(k), other], s.c_recv.at[k]).wait_recv()
@@ -353,7 +344,7 @@
 
     def detour_copy(k, d, i):
         ref = kvb.at[row_slot(k, d), core, DETOURS[i]]
-        return remote(ref, ref, s.r_send.at[i, k - 1, d - 1], s.r_recv.at[i, k - 1, d - 1], {"sp": sp + n_x, "tp": tp})
+        return remote(ref, ref, s.sent.at[0], s.r_recv.at[i, k - 1, d - 1], {"sp": sp + n_x, "tp": tp})
 
     def passes_detour(k, i):
         return (z + 1 < n_z) & detoured(k + 1, DETOURS[i], x)
@@ -410,10 +401,10 @@
     loads.q_gain.wait()
     own_normed = normed[core].reshape(half, n_tp * block)
     latq[core] = rms_rows(dot(own_normed, w.query_latent[...]), small.q_gain[...]).astype(BF16)
-    latq_copy = remote(latq.at[core], latq.at[core], s.q_sems.at[0], s.q_sems.at[1], to_sibling)
+    latq_copy = remote(latq.at[core], latq.at[core], s.sent.at[0], s.q_sems.at[0], to_sibling)
     latq_copy.start()
 
-    arrival(normed.at[other], s.n_sems.at[1]).wait_recv()
+    arrival(normed.at[other], s.n_sems.at[0]).wait_recv()
 
     if n_z > 2:
         take_second(0, 1)
@@ -430,9 +421,9 @@
     local_kv[...] = qkv[:, : 2 * kv_width]
     queries[...] = qkv[:, 2 * kv_width :]
     tail = local_kv.at[pl.ds(rows - WINDOW, WINDOW)]
-    halo_copy = remote(tail, halo, s.halo_sem.at[0], s.halo_sem.at[1], {"sp": sp + 1, "tp": tp})
-    turn_copy = remote(tail, turn, s.halo_sem.at[0], s.halo_sem.at[2], {"sp": z * n_x, "tp": tp})
-    relay_copy = remote(turn, halo, s.halo_sem.at[3], s.halo_sem.at[1], {"sp": sp + n_x, "tp": tp})
+    halo_copy = remote(tail, halo, s.sent.at[0], s.halo_sem.at[0], {"sp": sp + 1, "tp": tp})
+    turn_copy = remote(tail, turn, s.sent.at[0], s.halo_sem.at[1], {"sp": z * n_x, "tp": tp})
+    relay_copy = remote(turn, halo, s.sent.at[0], s.halo_sem.at[0], {"sp": sp + n_x, "tp": tp})
 
     @pl.when((x + 1 == n_x) & (z + 1 < n_z))
     def _():
@@ -441,7 +432,7 @@
     take_first(pieces - 2)
 
     def queries_up():
-        arrival(latq.at[other], s.q_sems.at[1]).wait_recv()
+        arrival(latq.at[other], s.q_sems.at[0]).wait_recv()
         loads.content.wait()
         loads.rotary.wait()
         latent_query = latq[...].reshape(rows, latent)
@@ -457,9 +448,13 @@
         loads.key_up.wait()
         loads.value_up.wait()
 
-    def attend(slot, diagonal):
-        source = kvb[slot, :, :, :piece, :].reshape(rows, latent)
-        rope_part = rope_rows(slot)
+    def attend(slot, diagonal, which=None):
+        if which is None:
+            source = kvb[slot, :, :, :piece, :].reshape(rows, latent)
+            rope_part = rope_rows(slot)
+        else:
+            source = kvb[slot, which, :, :piece, :].reshape(half, latent)
+            rope_part = rope_rows(slot, [which])
         keys = dot(source, w.key_up[...]).astype(BF16)
         values = dot(source, w.value_up[...]).astype(BF16)
         heads = range(lat_heads)
@@ -492,7 +487,7 @@
     def take_halo():
         @pl.when(sp > 0)
         def _():
-            arrival(halo, s.halo_sem.at[1]).wait_recv()
+            arrival(halo, s.halo_sem.at[0]).wait_recv()
 
         @pl.when(sp == 0)
         def _():
@@ -533,7 +528,7 @@
 
     def win_copy(i):
         ref = winb.at[core, win_rows[i]]
-        return remote(ref, ref, s.win_send.at[i], s.win_recv.at[i], to_sibling)
+        return remote(ref, ref, s.sent.at[0], s.win_recv.at[i], to_sibling)
 
     win_rows = (pl.ds(WINDOW, rows - WINDOW), pl.ds(0, WINDOW))
 
@@ -541,7 +536,7 @@
         return dot(winb[0, at], wcol[0, j]) + dot(winb[1, at], wcol[1, j])
 
     def part_copy(d, at):
-        return remote(psend.at[d - 1, at], precv.at[d - 1, at], s.p_send.at[d - 1], s.p_recv.at[d - 1],
+        return remote(psend.at[d - 1, at], precv.at[d - 1, at], s.sent.at[0], s.p_recv.at[d - 1],
                       {"sp": sp, "tp": lax.rem(y + d, n_y) * 2 + core})
 
     def window_parts(i):
@@ -578,7 +573,7 @@
     if n_z > 2:
         take_second(1, pieces // 2)
     pltpu.make_async_copy(wcol.at[core], wcol.at[core], s.w_sems.at[0]).wait()
-    arrival(wcol.at[other], s.w_sems.at[2]).wait_recv()
+    arrival(wcol.at[other], s.w_sems.at[1]).wait_recv()
     window_parts(0)
     take_rows(0)
     wait_column(0)
@@ -590,14 +585,17 @@
     def _():
         halo_copy.start()
 
+    @pl.when((x == 0) & (z + 1 < n_z))
+    def _():
+        arrival(turn, s.halo_sem.at[1]).wait_recv()
+        relay_copy.start()
+
 
     def take_pieces(k, lo, hi):
         @pl.when(z >= k)
         def _():
             for h in range(lo, hi):
                 take_column(k, h)
-
-    near = (x > 0) | (z == 0)
 
     def first_window():
         take_halo()
@@ -621,43 +619,43 @@
         def _():
             take_pieces(k, pieces - 1, pieces)
 
-            @pl.when((x == 0) & (z + 1 < n_z))
-            def _():
-                arrival(turn, s.halo_sem.at[2]).wait_recv()
-                relay_copy.start()
-
-        pl.when((k == 4) & near)(last_parts)
-        pl.when((k == 4) & ~near)(first_window)
+        pl.when(k == 4)(last_parts)
 
         @pl.when(k > 2)
         def _():
             pl.when(x == 0)(functools.partial(take_pieces, k, 0, 1))
             take_pieces(k, 1, pieces // 2)
 
-        @pl.when((z >= k - 1) & (k == n_z))
-        def _():
-            take_rows(k - 1)
-
-        pl.when((k == 4) & ~near)(last_parts)
-
         for d in range(1, n_x):
-            @pl.when((z >= k - 2) & takes_row(k - 2, d))
+            @pl.when((z >= k - 2) & takes_row(k - 2, d) & (k <= n_z))
             def _():
                 attend_row(k - 2, d)
 
+            @pl.when((z >= k - 2) & (k == n_z + 1))
+            def _():
+                def halves(i, _):
+                    @pl.when(i == 1)
+                    def _():
+                        wait_row(k - 2, d)
+
+                    attend(row_slot(k - 2, d), False, jnp.where(i == 0, core, other))
+                    return 0
+
+                lax.fori_loop(0, 2, halves, 0)
+
 
         @pl.when(k > 2)
         def _():
             take_pieces(k, pieces // 2, pieces - 1)
 
-        pl.when((k == 3) & near)(first_window)
+        pl.when(k == 3)(first_window)
 
         @pl.when(k > 2)
         def _():
             take_pieces(k, pieces - 1, pieces)
 
 
-        @pl.when((z >= k - 1) & (k != n_z))
+        @pl.when(z >= k - 1)
         def _():
             take_rows(k - 1)
 
@@ -673,18 +671,18 @@
     def gather(part):
         own = lat.at[tp, part]
         sends = [
-            remote(own, own, s.y_send.at[d - 1], s.y_recv.at[part, d - 1],
+            remote(own, own, s.sent.at[0], s.y_recv.at[part, d - 1],
                    {"sp": sp, "tp": lax.rem(y + d, n_y) * 2 + core})
             for d in range(1, n_y)
         ]
-        sends.append(remote(own, own, s.s_send.at[0], s.s_recv.at[part], to_sibling))
+        sends.append(remote(own, own, s.sent.at[0], s.s_recv.at[part], to_sibling))
         return sends
 
     def forward(part):
         for d in range(1, n_y):
             ref = lat.at[lax.rem(y + n_y - d, n_y) * 2 + core, part]
             arrival(ref, s.y_recv.at[part, d - 1]).wait_recv()
-            remote(ref, ref, s.s_send.at[d], s.s_recv.at[part], to_sibling).start()
+            remote(ref, ref, s.sent.at[0], s.s_recv.at[part], to_sibling).start()
 
     def arrived(part):
         arrival(lat.at[pl.ds(0, n_y), part], s.s_recv.at[part]).wait_recv()
@@ -722,18 +720,18 @@
     def leave(ref, send):
         remote(ref, ref, send, send, to_sibling).wait_send()
 
-    leave(ownf.at[pl.ds(0, half)], s.f_send.at[0])
+    leave(ownf.at[pl.ds(0, half)], s.sent.at[0])
     for d in range(1, n_y):
-        leave(ownf, s.f_send.at[d])
-    leave(normed.at[core], s.n_sems.at[0])
+        leave(ownf, s.sent.at[0])
+    leave(normed.at[core], s.sent.at[0])
     latq_copy.wait_send()
-    leave(wcol.at[core], s.w_sems.at[1])
-    leave(columns.at[tp], s.col_send.at[0])
+    leave(wcol.at[core], s.sent.at[0])
+    leave(columns.at[tp], s.sent.at[0])
 
     @when_across
     def _():
         for d in range(1, n_y):
-            leave(columns.at[pl.ds(0, 2)], s.col_send.at[d])
+            leave(columns.at[pl.ds(0, 2)], s.sent.at[0])
 
     if paired:
         for d in range(1, n_y):
@@ -741,10 +739,10 @@
     for i in range(2):
         win_copy(i).wait_send()
     for d in range(1, n_y):
-        leave(psend.at[d - 1], s.p_send.at[d - 1])
-        leave(lat.at[tp], s.y_send.at[d - 1])
-        leave(lat.at[tp], s.s_send.at[d])
-    leave(lat.at[tp], s.s_send.at[0])
+        leave(psend.at[d - 1], s.sent.at[0])
+        leave(lat.at[tp], s.sent.at[0])
+        leave(lat.at[tp], s.sent.at[0])
+    leave(lat.at[tp], s.sent.at[0])
 
     @pl.when((x + 1 < n_x) | (z + 1 < n_z))
     def _():
@@ -761,20 +759,20 @@
 
             @pl.when(z + 1 < n_z)
             def _():
-                leave(own, s.z_send.at[k])
-
-            leave(own, s.c_send.at[k])
+                leave(own, s.sent.at[0])
+
+            leave(own, s.sent.at[0])
             for d in range(1, n_x):
                 to = lax.rem(x + d, n_x)
                 fewer = [detoured(k, h, to) for h in DETOURS]
 
                 @pl.when(sends_row(k, d) & ~(fewer[0] | fewer[1]))
                 def _():
-                    leave(own, s.x_send.at[k, d - 1])
+                    leave(own, s.sent.at[0])
 
                 @pl.when(fewer[0] | fewer[1])
                 def _():
-                    leave(own.at[pl.ds(0, pieces - 1)], s.x_send.at[k, d - 1])
+                    leave(own.at[pl.ds(0, pieces - 1)], s.sent.at[0])
 
                 for i in range(2):
                     @pl.when(takes_row(k, d) & passes_detour(k, i))
@@ -783,7 +781,7 @@
 
                 @pl.when(takes_row(k, d))
                 def _():
-                    leave(own, s.d_send.at[k, d - 1])
+                    leave(own, s.sent.at[0])
 
         return 0
 
@@ -842,36 +840,25 @@
         cosine=vm((2, pieces, piece, ROPE), F32),
         sine=vm((2, pieces, piece, ROPE), F32),
         own_sem=dma((2,)),
+        sent=dma((1,)),
         small_sem=dma((len(SMALL),)),
         w_sem=dma((len(weights),)),
-        f_send=dma((n_y,)),
         f_recv=dma((pieces,)),
-        n_sems=dma((2,)),
-        q_sems=dma((2,)),
-        w_sems=dma((3,)),
+        n_sems=dma((1,)),
+        q_sems=dma((1,)),
+        w_sems=dma((2,)),
         col_own=dma((1,)),
-        col_send=dma((n_y,)),
         col_recv=dma((n_y,)),
-        pair_send=dma((n_y - 1,)),
         pair_recv=dma((n_y - 1,)),
-        halo_sem=dma((4,)),
-        win_send=dma((2,)),
+        halo_sem=dma((2,)),
         win_recv=dma((2,)),
-        p_send=dma((n_y - 1,)),
         p_recv=dma((n_y - 1,)),
-        y_send=dma((n_y - 1,)),
         y_recv=dma((out_parts, n_y - 1)),
-        s_send=dma((n_y,)),
         s_recv=dma((out_parts,)),
-        z_send=dma((n_z - 1,)),
         z_recv=dma((pieces, n_z - 1)),
-        r_send=dma((2, n_z - 2, n_x - 1)),
         r_recv=dma((2, n_z - 2, n_x - 1)),
-        x_send=dma((n_z, n_x - 1)),
         x_recv=dma((pieces, n_z, n_x - 1)),
-        c_send=dma((n_z,)),
         c_recv=dma((n_z,)),
-        d_send=dma((n_z, n_x - 1)),
         d_recv=dma((n_z, n_x - 1)),
     )
     return pl.pallas_call(

time: 41.1 us -> 40.4 us (0.983)
  Pallas kernels: 40.2 us -> 39.5 us
    pallas_call x1, Pallas kernels: 40.2 us -> 39.5 us  [on_device(): pl.pallas_call(functools.partial(kernel, dims, tuple(scratch)), out_shape...]
where the time goes in v4:
time: 40.4 us; the launch traced here: 40.2 us
  Pallas kernels  39.5 us (98%)
  local copies, waits for them, and re-layouts  0.75 us (2%)
    pallas_call x1, Pallas kernels, on_device(): pl.pallas_call(functools.partial(kernel, dims, tuple(scratch)), out_shape...  39.5 us

profile of v4, /device:TPU:25, one launch (start us, length us, event | category | flops | bytes accessed | tf_op | source)
XLA Modules:
  0.0 40.2 jit_solution(949293613903591067)
XLA Ops:
  0.0 39.5 %shard_map.190 = bf16[384,512]{1,0:T(8,128)(2,1)S(1)} custom-call(bf16[384,512]{1,0:T(8,128)(2,1)} %refs_0_.1, f32[1,2048]{1,0:T(1,128)} %bitcast.6, f32[1,4]{1,0:T(1,128)} %bitcast.9, f32[1,512]{1,0:T(1,128)} %bitcast.7, f32[1,512]{1,0:T(1,128)} %bitcast.8, f32[1,64]{1,0:T(1,128)} %constant.2.clone.refs_5_, bf16[2048,512]{1,0:T(8,128)(2,1)} %refs_6_.1, ...), custom_call_target="tpu_custom_call" | custom-call | tf_op jit(solution)/shard_map/pallas_call | solution.py:864
  39.5 0.7 %copy.22 = bf16[384,512]{1,0:T(8,128)(2,1)} copy(bf16[384,512]{1,0:T(8,128)(2,1)S(1)} %shard_map.190) | data formatting | bytes 786432

commit v5 on v4

--- a/solution.py
+++ b/solution.py
@@ -59,6 +59,7 @@
     return types.SimpleNamespace(**dict(zip(names, values)))
 
 
+UP = ("key_up", "value_up")
 MERGED = ("key", "value", "query")
 
 
@@ -180,7 +181,11 @@
     first = 0
     for i, name in enumerate(WEIGHTS):
         source = getattr(w_hbm, name)
-        if name in kept:
+        if name == "key_up":
+            to = s.up.at[:, pl.ds(0, lat_heads * NOPE)]
+        elif name == "value_up":
+            to = s.up.at[:, pl.ds(lat_heads * NOPE, lat_heads * VDIM)]
+        elif name in kept:
             to = getattr(w, name)
         else:
             to = s.w_qkv.at[:, pl.ds(first, source.shape[1])]
@@ -296,15 +301,15 @@
 
     def x_copy(k, d, h):
         ref = kvb.at[column_slot(k), core, h]
-        return remote(ref, ref, s.sent.at[0], s.x_recv.at[h, k, d - 1],
+        return remote(ref, ref, s.sent.at[0], s.x_recv.at[k, d - 1],
                       {"sp": z * n_x + lax.rem(x + d, n_x), "tp": tp})
 
     def c_copy(k, h):
         ref = kvb.at[column_slot(k), core, h]
         return remote(ref, ref, s.sent.at[0], s.c_recv.at[k], to_sibling)
 
-    def d_copy(k, d, h):
-        ref = kvb.at[row_slot(k, d), core, h]
+    def d_copy(k, d):
+        ref = kvb.at[row_slot(k, d), core]
         return remote(ref, ref, s.sent.at[0], s.d_recv.at[k, d - 1], to_sibling)
 
     def wait_column(k):
@@ -349,26 +354,28 @@
     def passes_detour(k, i):
         return (z + 1 < n_z) & detoured(k + 1, DETOURS[i], x)
 
-    def take_row(k, h):
-        for d in range(1, n_x):
-            def from_x():
-                arrival(kvb.at[row_slot(k, d), core, h], s.x_recv.at[h, k, d - 1]).wait_recv()
-
-            def from_z():
-                arrival(kvb.at[row_slot(k, d), core, h], s.r_recv.at[DETOURS.index(h), k - 2, d - 1]).wait_recv()
-
-            @pl.when(takes_row(k, d))
+    def take_row(k, d):
+        own = kvb.at[row_slot(k, d), core]
+        shorter = functools.reduce(jnp.logical_or, [detoured(k, h, x) for h in DETOURS])
+
+        @pl.when(~shorter)
+        def _():
+            arrival(own, s.x_recv.at[k, d - 1]).wait_recv()
+
+        @pl.when(shorter)
+        def _():
+            arrival(own.at[pl.ds(0, pieces - 1)], s.x_recv.at[k, d - 1]).wait_recv()
+
+        for i, h in enumerate(DETOURS):
+            @pl.when(detoured(k, h, x))
             def _():
-                if h in DETOURS:
-                    pl.when(~detoured(k, h, x))(from_x)
-                    pl.when(detoured(k, h, x))(from_z)
-
-                    @pl.when(passes_detour(k, DETOURS.index(h)))
-                    def _():
-                        detour_copy(k, d, DETOURS.index(h)).start()
-                else:
-                    from_x()
-                d_copy(k, d, h).start()
+                arrival(own.at[h], s.r_recv.at[i, k - 2, d - 1]).wait_recv()
+
+            @pl.when(passes_detour(k, i))
+            def _():
+                detour_copy(k, d, i).start()
+
+        d_copy(k, d).start()
 
     def take_second(lo, hi):
         for h in range(lo, hi):
@@ -455,8 +462,8 @@
         else:
             source = kvb[slot, which, :, :piece, :].reshape(half, latent)
             rope_part = rope_rows(slot, [which])
-        keys = dot(source, w.key_up[...]).astype(BF16)
-        values = dot(source, w.value_up[...]).astype(BF16)
+        both = dot(source, s.up[...]).astype(BF16)
+        keys, values = both[:, : lat_heads * NOPE], both[:, lat_heads * NOPE :]
         heads = range(lat_heads)
         scores = []
         for h in heads:
@@ -558,8 +565,8 @@
         lax.fori_loop(0, block // 256, step, 0)
 
     def take_rows(k):
-        for h in range(pieces):
-            take_row(k, h)
+        for d in range(1, n_x):
+            pl.when(takes_row(k, d))(functools.partial(take_row, k, d))
 
     def attend_row(k, d):
         wait_row(k, d)
@@ -605,16 +612,31 @@
     def last_parts():
         window_parts(1)
 
+    def attend_halves(slot, wait):
+        def halves(i, _):
+            @pl.when(i == 1)
+            def _():
+                wait()
+
+            attend(slot, False, jnp.where(i == 0, core, other))
+            return 0
+
+        lax.fori_loop(0, 2, halves, 0)
+
     def step(k, _):
         @pl.when(k == 4 - parity)
         def _():
             pair_forward()
 
-        @pl.when(z >= k - 1)
+        @pl.when((z >= k - 1) & (k < n_z))
         def _():
             wait_column(k - 1)
             attend(column_slot(k - 1), False)
 
+        @pl.when((z >= k - 1) & (k == n_z))
+        def _():
+            attend_halves(column_slot(k - 1), functools.partial(wait_column, k - 1))
+
         @pl.when(k == 2)
         def _():
             take_pieces(k, pieces - 1, pieces)
@@ -627,45 +649,39 @@
             take_pieces(k, 1, pieces // 2)
 
         for d in range(1, n_x):
-            @pl.when((z >= k - 2) & takes_row(k - 2, d) & (k <= n_z))
+            @pl.when((z >= k - 2) & takes_row(k - 2, d))
             def _():
                 attend_row(k - 2, d)
 
-            @pl.when((z >= k - 2) & (k == n_z + 1))
+        @pl.when(k > 2)
+        def _():
+            take_pieces(k, pieces // 2, pieces - 1)
+
+        pl.when(k == 3)(first_window)
+
+        @pl.when(k > 2)
+        def _():
+            take_pieces(k, pieces - 1, pieces)
+
+
+        @pl.when(z >= k - 1)
+        def _():
+            take_rows(k - 1)
+
+        @pl.when(x > 0)
+        def _():
+            take_pieces(k + 1, 0, 1)
+
+        return 0
+
+    lax.fori_loop(2, max(n_z, 4) + 1, step, 0)
+
+    @pl.when(z == n_z - 1)
+    def _():
+        for d in range(1, n_x):
+            @pl.when(takes_row(n_z - 1, d))
             def _():
-                def halves(i, _):
-                    @pl.when(i == 1)
-                    def _():
-                        wait_row(k - 2, d)
-
-                    attend(row_slot(k - 2, d), False, jnp.where(i == 0, core, other))
-                    return 0
-
-                lax.fori_loop(0, 2, halves, 0)
-
-
-        @pl.when(k > 2)
-        def _():
-            take_pieces(k, pieces // 2, pieces - 1)
-
-        pl.when(k == 3)(first_window)
-
-        @pl.when(k > 2)
-        def _():
-            take_pieces(k, pieces - 1, pieces)
-
-
-        @pl.when(z >= k - 1)
-        def _():
-            take_rows(k - 1)
-
-        @pl.when(x > 0)
-        def _():
-            take_pieces(k + 1, 0, 1)
-
-        return 0
-
-    lax.fori_loop(2, max(n_z, 3) + 2, step, 0)
+                attend_halves(row_slot(n_z - 1, d), functools.partial(wait_row, n_z - 1, d))
 
 
     def gather(part):
@@ -691,7 +707,7 @@
         at = slice(part * out_rows, (part + 1) * out_rows)
         for h in range(lat_heads):
             lat[tp, part, :, h * VDIM : (h + 1) * VDIM] = (
-                acc[h, :, at] / total[h, :, at]).T.astype(BF16)
+                acc[h, :, at] * (1.0 / total[h, :, at])).T.astype(BF16)
         start(gather(part))
     gate(0)
     gate(1)
@@ -815,7 +831,8 @@
     vm = pltpu.VMEM
     scratch = dict(
         **{"small_" + n: (pltpu.SMEM if n == "sinks" else vm)(a.shape, F32) for n, a in zip(SMALL, smalls)},
-        **{"w_" + n: vm(a.shape, BF16) for n, a in zip(WEIGHTS, weights) if not (merge and n in MERGED)},
+        **{"w_" + n: vm(a.shape, BF16) for n, a in zip(WEIGHTS, weights) if not (merge and n in MERGED or n in UP)},
+        up=vm((latent, w_key_up.shape[1] + w_value_up.shape[1]), BF16),
         **(dict(w_qkv=vm((width, 2 * w_key.shape[1] + w_query.shape[1]), BF16)) if merge else {}),
         ownf=vm((rows, block), BF16),
         feat=vm((n_tp, rows // 2, block), BF16),
@@ -857,7 +874,7 @@
         s_recv=dma((out_parts,)),
         z_recv=dma((pieces, n_z - 1)),
         r_recv=dma((2, n_z - 2, n_x - 1)),
-        x_recv=dma((pieces, n_z, n_x - 1)),
+        x_recv=dma((n_z, n_x - 1)),
         c_recv=dma((n_z,)),
         d_recv=dma((n_z, n_x - 1)),
     )

time: 40.4 us -> 39.9 us (0.988)
  Pallas kernels: 39.5 us -> 39 us
    pallas_call x1, Pallas kernels: 39.5 us -> 39 us  [on_device(): pl.pallas_call(functools.partial(kernel, dims, tuple(scratch)), out_shape...]
where the time goes in v5:
time: 39.9 us; the launch traced here: 39.8 us
  Pallas kernels  39 us (98%)
  local copies, waits for them, and re-layouts  0.75 us (2%)
    pallas_call x1, Pallas kernels, on_device(): pl.pallas_call(functools.partial(kernel, dims, tuple(scratch)), out_shape...  39 us

profile of v5, /device:TPU:25, one launch (start us, length us, event | category | flops | bytes accessed | tf_op | source)
XLA Modules:
  0.0 39.8 jit_solution(8083121635374860407)
XLA Ops:
  0.0 39.0 %shard_map.190 = bf16[384,512]{1,0:T(8,128)(2,1)S(1)} custom-call(bf16[384,512]{1,0:T(8,128)(2,1)} %refs_0_.1, f32[1,2048]{1,0:T(1,128)} %bitcast.6, f32[1,4]{1,0:T(1,128)} %bitcast.9, f32[1,512]{1,0:T(1,128)} %bitcast.7, f32[1,512]{1,0:T(1,128)} %bitcast.8, f32[1,64]{1,0:T(1,128)} %constant.2.clone.refs_5_, bf16[2048,512]{1,0:T(8,128)(2,1)} %refs_6_.1, ...), custom_call_target="tpu_custom_call" | custom-call | tf_op jit(solution)/shard_map/pallas_call | solution.py:881
  39.0 0.7 %copy.22 = bf16[384,512]{1,0:T(8,128)(2,1)} copy(bf16[384,512]{1,0:T(8,128)(2,1)S(1)} %shard_map.190) | data formatting | bytes 786432

commit v6 on v5

--- a/solution.py
+++ b/solution.py
@@ -121,6 +121,24 @@
     def feat_rows(j, h):
         return feat.at[j, pl.ds(h * piece, piece)]
 
+    barrier = pltpu.get_barrier_semaphore()
+
+    def greet(where):
+        pl.semaphore_signal(barrier, inc=1, device_id=where, device_id_type=MESH)
+
+    for d in range(1, n_tp):
+        greet({"sp": sp, "tp": lax.rem(tp + d, n_tp)})
+    for d in range(1, n_x):
+        greet({"sp": z * n_x + lax.rem(x + d, n_x), "tp": tp})
+
+    @pl.when(z + 1 < n_z)
+    def _():
+        greet({"sp": sp + n_x, "tp": tp})
+
+    @pl.when(z > 0)
+    def _():
+        greet({"sp": sp - n_x, "tp": tp})
+
     own_load = [
         pltpu.make_async_copy(features, ownf, s.own_sem.at[0]),
         pltpu.make_async_copy(
@@ -133,24 +151,6 @@
     ])
     for name in SMALL:
         getattr(loads, name).start()
-
-    barrier = pltpu.get_barrier_semaphore()
-
-    def greet(where):
-        pl.semaphore_signal(barrier, inc=1, device_id=where, device_id_type=MESH)
-
-    for d in range(1, n_tp):
-        greet({"sp": sp, "tp": lax.rem(tp + d, n_tp)})
-    for d in range(1, n_x):
-        greet({"sp": z * n_x + lax.rem(x + d, n_x), "tp": tp})
-
-    @pl.when(z + 1 < n_z)
-    def _():
-        greet({"sp": sp + n_x, "tp": tp})
-
-    @pl.when(z > 0)
-    def _():
-        greet({"sp": sp - n_x, "tp": tp})
 
     one, none = jnp.int32(1), jnp.int32(0)
     pl.semaphore_wait(
@@ -687,18 +687,18 @@
     def gather(part):
         own = lat.at[tp, part]
         sends = [
-            remote(own, own, s.sent.at[0], s.y_recv.at[part, d - 1],
+            remote(own, own, s.sent.at[1], s.y_recv.at[part, d - 1],
                    {"sp": sp, "tp": lax.rem(y + d, n_y) * 2 + core})
             for d in range(1, n_y)
         ]
-        sends.append(remote(own, own, s.sent.at[0], s.s_recv.at[part], to_sibling))
+        sends.append(remote(own, own, s.sent.at[1], s.s_recv.at[part], to_sibling))
         return sends
 
     def forward(part):
         for d in range(1, n_y):
             ref = lat.at[lax.rem(y + n_y - d, n_y) * 2 + core, part]
             arrival(ref, s.y_recv.at[part, d - 1]).wait_recv()
-            remote(ref, ref, s.sent.at[0], s.s_recv.at[part], to_sibling).start()
+            remote(ref, ref, s.sent.at[1], s.s_recv.at[part], to_sibling).start()
 
     def arrived(part):
         arrival(lat.at[pl.ds(0, n_y), part], s.s_recv.at[part]).wait_recv()
@@ -724,6 +724,73 @@
             arrival(columns.at[base + 1 - parity], s.pair_recv.at[d - 1]).wait_recv()
         else:
             arrival(columns.at[pl.ds(base, 2)], s.col_recv.at[d]).wait_recv()
+    def leave(ref, send):
+        remote(ref, ref, send, send, to_sibling).wait_send()
+
+    leave(ownf.at[pl.ds(0, half)], s.sent.at[0])
+    for d in range(1, n_y):
+        leave(ownf, s.sent.at[0])
+    leave(normed.at[core], s.sent.at[0])
+    latq_copy.wait_send()
+    leave(wcol.at[core], s.sent.at[0])
+    leave(columns.at[tp], s.sent.at[0])
+
+    @when_across
+    def _():
+        for d in range(1, n_y):
+            leave(columns.at[pl.ds(0, 2)], s.sent.at[0])
+
+    if paired:
+        for d in range(1, n_y):
+            pair_copy(d).wait_send()
+    for i in range(2):
+        win_copy(i).wait_send()
+    for d in range(1, n_y):
+        leave(psend.at[d - 1], s.sent.at[0])
+
+    @pl.when((x + 1 < n_x) | (z + 1 < n_z))
+    def _():
+        halo_copy.wait_send()
+
+    @pl.when((x == 0) & (z + 1 < n_z))
+    def _():
+        relay_copy.wait_send()
+
+    def drain(k, _):
+        @pl.when(z >= k)
+        def _():
+            own = kvb.at[column_slot(k), core]
+
+            @pl.when(z + 1 < n_z)
+            def _():
+                leave(own, s.sent.at[0])
+
+            leave(own, s.sent.at[0])
+            for d in range(1, n_x):
+                to = lax.rem(x + d, n_x)
+                fewer = [detoured(k, h, to) for h in DETOURS]
+
+                @pl.when(sends_row(k, d) & ~(fewer[0] | fewer[1]))
+                def _():
+                    leave(own, s.sent.at[0])
+
+                @pl.when(fewer[0] | fewer[1])
+                def _():
+                    leave(own.at[pl.ds(0, pieces - 1)], s.sent.at[0])
+
+                for i in range(2):
+                    @pl.when(takes_row(k, d) & passes_detour(k, i))
+                    def _():
+                        detour_copy(k, d, i).wait_send()
+
+                @pl.when(takes_row(k, d))
+                def _():
+                    leave(own, s.sent.at[0])
+
+        return 0
+
+    lax.fori_loop(0, n_z, drain, 0)
+
     for part in range(out_parts):
         at = slice(part * out_rows, (part + 1) * out_rows)
         forward(part)
@@ -733,75 +800,8 @@
             latent_branch = latent_branch + dot(lat[j, part], columns[j])
         out[at, :] = (gates[0, at] + gates[1, at] * latent_branch).astype(BF16)
 
-    def leave(ref, send):
-        remote(ref, ref, send, send, to_sibling).wait_send()
-
-    leave(ownf.at[pl.ds(0, half)], s.sent.at[0])
-    for d in range(1, n_y):
-        leave(ownf, s.sent.at[0])
-    leave(normed.at[core], s.sent.at[0])
-    latq_copy.wait_send()
-    leave(wcol.at[core], s.sent.at[0])
-    leave(columns.at[tp], s.sent.at[0])
-
-    @when_across
-    def _():
-        for d in range(1, n_y):
-            leave(columns.at[pl.ds(0, 2)], s.sent.at[0])
-
-    if paired:
-        for d in range(1, n_y):
-            pair_copy(d).wait_send()
-    for i in range(2):
-        win_copy(i).wait_send()
-    for d in range(1, n_y):
-        leave(psend.at[d - 1], s.sent.at[0])
-        leave(lat.at[tp], s.sent.at[0])
-        leave(lat.at[tp], s.sent.at[0])
-    leave(lat.at[tp], s.sent.at[0])
-
-    @pl.when((x + 1 < n_x) | (z + 1 < n_z))
-    def _():
-        halo_copy.wait_send()
-
-    @pl.when((x == 0) & (z + 1 < n_z))
-    def _():
-        relay_copy.wait_send()
-
-    def drain(k, _):
-        @pl.when(z >= k)
-        def _():
-            own = kvb.at[column_slot(k), core]
-
-            @pl.when(z + 1 < n_z)
-            def _():
-                leave(own, s.sent.at[0])
-
-            leave(own, s.sent.at[0])
-            for d in range(1, n_x):
-                to = lax.rem(x + d, n_x)
-                fewer = [detoured(k, h, to) for h in DETOURS]
-
-                @pl.when(sends_row(k, d) & ~(fewer[0] | fewer[1]))
-                def _():
-                    leave(own, s.sent.at[0])
-
-                @pl.when(fewer[0] | fewer[1])
-                def _():
-                    leave(own.at[pl.ds(0, pieces - 1)], s.sent.at[0])
-
-                for i in range(2):
-                    @pl.when(takes_row(k, d) & passes_detour(k, i))
-                    def _():
-                        detour_copy(k, d, i).wait_send()
-
-                @pl.when(takes_row(k, d))
-                def _():
-                    leave(own, s.sent.at[0])
-
-        return 0
-
-    lax.fori_loop(0, n_z, drain, 0)
+    for _ in range(n_y + n_y - 1):
+        leave(lat.at[tp], s.sent.at[1])
 
 
 def on_device(dims, features, norm_gain, w_query, w_key, w_value, head_sinks, w_query_latent,
@@ -857,7 +857,7 @@
         cosine=vm((2, pieces, piece, ROPE), F32),
         sine=vm((2, pieces, piece, ROPE), F32),
         own_sem=dma((2,)),
-        sent=dma((1,)),
+        sent=dma((2,)),
         small_sem=dma((len(SMALL),)),
         w_sem=dma((len(weights),)),
         f_recv=dma((pieces,)),

time: 39.9 us -> 39.8 us (level)
  no operation moved by 1% of the time
where the time goes in v6:
time: 39.8 us; the launch traced here: 39.6 us
  Pallas kernels  38.8 us (97%)
  local copies, waits for them, and re-layouts  0.75 us (2%)
    pallas_call x1, Pallas kernels, on_device(): pl.pallas_call(functools.partial(kernel, dims, tuple(scratch)), out_shape...  38.8 us

profile of v6, /device:TPU:25, one launch (start us, length us, event | category | flops | bytes accessed | tf_op | source)
XLA Modules:
  0.0 39.6 jit_solution(8430668162039427831)
XLA Ops:
  0.0 38.8 %shard_map.190 = bf16[384,512]{1,0:T(8,128)(2,1)S(1)} custom-call(bf16[384,512]{1,0:T(8,128)(2,1)} %refs_0_.1, f32[1,2048]{1,0:T(1,128)} %bitcast.6, f32[1,4]{1,0:T(1,128)} %bitcast.9, f32[1,512]{1,0:T(1,128)} %bitcast.7, f32[1,512]{1,0:T(1,128)} %bitcast.8, f32[1,64]{1,0:T(1,128)} %constant.2.clone.refs_5_, bf16[2048,512]{1,0:T(8,128)(2,1)} %refs_6_.1, ...), custom_call_target="tpu_custom_call" | custom-call | tf_op jit(solution)/shard_map/pallas_call | solution.py:881
  38.8 0.7 %copy.22 = bf16[384,512]{1,0:T(8,128)(2,1)} copy(bf16[384,512]{1,0:T(8,128)(2,1)S(1)} %shard_map.190) | data formatting | bytes 786432

commit v7 on v6

--- a/solution.py
+++ b/solution.py
@@ -179,6 +179,8 @@
         start(feature_sends(h))
 
     first = 0
+    slots = [i for i, name in enumerate(WEIGHTS) if name in kept and name not in UP]
+    slots += [WEIGHTS.index(UP[0])] + [WEIGHTS.index(MERGED[0])] * merged
     for i, name in enumerate(WEIGHTS):
         source = getattr(w_hbm, name)
         if name == "key_up":
@@ -190,7 +192,8 @@
         else:
             to = s.w_qkv.at[:, pl.ds(first, source.shape[1])]
             first += source.shape[1]
-        copy = pltpu.make_async_copy(source, to, s.w_sem.at[i])
+        shared = WEIGHTS.index(UP[0]) if name in UP else i if name in kept else WEIGHTS.index(MERGED[0])
+        copy = pltpu.make_async_copy(source, to, s.w_sem.at[slots.index(shared)])
         copy.start()
         setattr(loads, name, copy)
 
@@ -419,8 +422,12 @@
     def all_normed():
         return normed[...].reshape(rows, n_tp * block)
 
-    for name in MERGED:
-        getattr(loads, name).wait()
+    if merged:
+        sem = s.w_sem.at[slots.index(WEIGHTS.index(MERGED[0]))]
+        pltpu.make_async_copy(s.w_qkv, s.w_qkv, sem).wait()
+    else:
+        for name in MERGED:
+            getattr(loads, name).wait()
     if merged:
         qkv = dot(all_normed(), s.w_qkv[...]).astype(BF16)
     else:
@@ -452,8 +459,7 @@
             turned = turned * cos_all + swap_halves(turned) * sin_all
             q_full[h, :NOPE, :] = content[:, h * NOPE : (h + 1) * NOPE].T.astype(BF16)
             q_full[h, NOPE:, :] = jnp.concatenate([turned, padding], axis=1).T.astype(BF16)
-        loads.key_up.wait()
-        loads.value_up.wait()
+        pltpu.make_async_copy(s.up, s.up, s.w_sem.at[slots.index(WEIGHTS.index(UP[0]))]).wait()
 
     def attend(slot, diagonal, which=None):
         if which is None:
@@ -584,18 +590,18 @@
     window_parts(0)
     take_rows(0)
     wait_column(0)
-    attend(sp, True)
-    if n_z > 2:
-        take_second(pieces // 2, pieces - 1)
-
-    @pl.when(x + 1 < n_x)
-    def _():
-        halo_copy.start()
-
     @pl.when((x == 0) & (z + 1 < n_z))
     def _():
         arrival(turn, s.halo_sem.at[1]).wait_recv()
         relay_copy.start()
+
+    attend(sp, True)
+    if n_z > 2:
+        take_second(pieces // 2, pieces - 1)
+
+    @pl.when(x + 1 < n_x)
+    def _():
+        halo_copy.start()
 
 
     def take_pieces(k, lo, hi):
@@ -859,7 +865,7 @@
         own_sem=dma((2,)),
         sent=dma((2,)),
         small_sem=dma((len(SMALL),)),
-        w_sem=dma((len(weights),)),
+        w_sem=dma((len(weights) - 1 - 2 * merge,)),
         f_recv=dma((pieces,)),
         n_sems=dma((1,)),
         q_sems=dma((1,)),

time: 39.8 us -> 39.9 us (level)
  no operation moved by 1% of the time
where the time goes in v7:
time: 39.9 us; the launch traced here: 39.7 us
  Pallas kernels  39 us (98%)
  local copies, waits for them, and re-layouts  0.75 us (2%)
    pallas_call x1, Pallas kernels, on_device(): pl.pallas_call(functools.partial(kernel, dims, tuple(scratch)), out_shape...  39 us

profile of v7, /device:TPU:25, one launch (start us, length us, event | category | flops | bytes accessed | tf_op | source)
XLA Modules:
  0.0 39.7 jit_solution(17402343121116280469)
XLA Ops:
  0.0 39.0 %shard_map.190 = bf16[384,512]{1,0:T(8,128)(2,1)S(1)} custom-call(bf16[384,512]{1,0:T(8,128)(2,1)} %refs_0_.1, f32[1,2048]{1,0:T(1,128)} %bitcast.6, f32[1,4]{1,0:T(1,128)} %bitcast.9, f32[1,512]{1,0:T(1,128)} %bitcast.7, f32[1,512]{1,0:T(1,128)} %bitcast.8, f32[1,64]{1,0:T(1,128)} %constant.2.clone.refs_5_, bf16[2048,512]{1,0:T(8,128)(2,1)} %refs_6_.1, ...), custom_call_target="tpu_custom_call" | custom-call | tf_op jit(solution)/shard_map/pallas_call | solution.py:887
  39.0 0.7 %copy.22 = bf16[384,512]{1,0:T(8,128)(2,1)} copy(bf16[384,512]{1,0:T(8,128)(2,1)S(1)} %shard_map.190) | data formatting | bytes 786432
